TPU v7x, 32 devices: a whole 2x2x4 slice. The times are simulated.
32 devices in a mesh: sp: 16 (over z, y, x), tp: 2 (over core).
Axes of the slice: x: 2, y: 2, z: 4, core: 2. Of those that a mesh axis runs over, the one named last changes fastest.
Arguments:
- tokens: bfloat16 [4096, 4096], P('sp', 'tp'), may hold values from -480 to 480
- gain: float32 [4096], P('tp'), may hold values from 0.1 to 1.9
- q_att: bfloat16 [4096, 2048], P('sp', 'tp'), may hold values from -2.90625 to 2.90625
- k_att: bfloat16 [4096, 1024], P('sp', 'tp'), may hold values from -0.09375 to 0.09375
- v_att: bfloat16 [4096, 1024], P('sp', 'tp'), may hold values from -0.75 to 0.75
- q_ret: bfloat16 [4096, 1024], P('sp', 'tp'), may hold values from -0.09375 to 0.09375
- k_ret: bfloat16 [4096, 1024], P('sp', 'tp'), may hold values from -0.09375 to 0.09375
- v_ret: bfloat16 [4096, 1024], P('sp', 'tp'), may hold values from -0.09375 to 0.09375
- out_att: bfloat16 [2048, 4096], P('tp', 'sp'), may hold values from -0.109375 to 0.109375
- out_ret: bfloat16 [1024, 4096], P('tp', 'sp'), may hold values from -0.109375 to 0.109375
- sink: float32 [16], P('tp'), may hold values from 3 to 7
- decay_log: float32 [8, 4096], P('tp', 'sp'), may hold values from -2.125 to 0
Outputs:
- mixed: bfloat16 [4096, 4096], P(('sp', 'tp'))
- log_weight: float32 [16, 4096], P('tp', 'sp')
All inputs are finite; a program needn't handle non-finite values.
Results may differ from a plain program's by a relative error of at most 0.017.
Values may be sent and summed in bfloat16 or wider, within the bound.
A program may use at most 128 MiB of HBM per device.

v0:
```python
import jax
import jax.numpy as jnp
from jax import lax
from jax.sharding import PartitionSpec as P

D = 4096
HEAD_DIM = 128
SPAN_RADIUS = 128


def with_halo(shard, sides, width):
    for axis, dim in sides:
        peers, length = (lax.axis_size(axis), shard.shape[dim])
        up = [(i, (i + 1) % peers) for i in range(peers - 1)]
        down = [(j, i) for i, j in up]
        last = lax.slice_in_dim(shard, length - width, length, axis=dim)
        initial = lax.slice_in_dim(shard, 0, width, axis=dim)
        before = lax.ppermute(last, axis, up)
        after = lax.ppermute(initial, axis, down)
        shard = jnp.concatenate([before, shard, after], axis=dim)
    return shard


def entering(shard, axis, combine, identity, reverse):
    peers, index = (lax.axis_size(axis), lax.axis_index(axis))
    everything = jax.tree.map(
        lambda part, kind: lax.all_gather(part.astype(kind), axis),
        shard,
        (jnp.bfloat16, jnp.bfloat16),
    )
    start = jax.tree.map(
        lambda part, zero: jnp.broadcast_to(jnp.asarray(zero, part.dtype), part.shape),
        shard,
        identity,
    )

    def turn(k, before):
        at = peers - 1 - k if reverse else k
        reached = at > index if reverse else at < index
        new = combine(
            before, jax.tree.map(lambda part, own: part[at].astype(own.dtype), everything, shard)
        )
        return jax.tree.map(lambda a, b: jnp.where(reached, a, b), new, before)

    return lax.fori_loop(0, peers, turn, start)


def rotate(values, angles):
    half = values.shape[-1] // 2
    first = values[..., :half]
    second = values[..., half:]
    cosine = jnp.cos(angles)[:, None, :]
    sine = jnp.sin(angles)[:, None, :]
    return jnp.concatenate(
        [first * cosine - second * sine, second * cosine + first * sine], axis=-1
    )


def fold_with(weights, piece):
    return tuple((jnp.dot(piece, weight, preferred_element_type=jnp.float32) for weight in weights))


def chain(earlier, later):
    return (earlier[0] * later[0], later[0][:, None, None] * earlier[1] + later[1])


def shards(
    tokens, gain, q_att, k_att, v_att, q_ret, k_ret, v_ret, out_att, out_ret, sink, decay_log
):
    tok_rows = tokens.shape[0]
    att_local = sink.shape[0]
    nearby_memory = k_att.shape[1] // HEAD_DIM
    ret_local = q_ret.shape[1] // HEAD_DIM
    group = att_local // nearby_memory
    total_rows = tok_rows * lax.axis_size("sp")
    offset = lax.axis_index("sp") * tok_rows
    highest = lax.Precision.HIGHEST
    widened = tokens.astype(jnp.float32)
    squares = lax.psum(jnp.sum(widened * widened, axis=1), "tp")
    inverse = lax.rsqrt(squares / D + 1e-06)[:, None]
    scaled = (widened * gain).astype(jnp.bfloat16)
    wide_qa, wide_ka, wide_va, wide_qr, wide_kr, wide_vr = (
        lax.all_gather(q_att, "sp", axis=0, tiled=True),
        lax.all_gather(k_att, "sp", axis=0, tiled=True),
        lax.all_gather(v_att, "sp", axis=0, tiled=True),
        lax.all_gather(q_ret, "sp", axis=0, tiled=True),
        lax.all_gather(k_ret, "sp", axis=0, tiled=True),
        lax.all_gather(v_ret, "sp", axis=0, tiled=True),
    )
    every_weight = (wide_qa, wide_ka, wide_va, wide_qr, wide_kr, wide_vr)
    proj_qa, proj_ka, proj_va, proj_qr, proj_kr, proj_vr = fold_with(
        every_weight, lax.all_gather(scaled, "tp", axis=1, tiled=True)
    )
    positions = (offset + jnp.arange(tok_rows, dtype=jnp.int32)).astype(jnp.float32)
    freqs = 10000.0 ** (-jnp.arange(0, HEAD_DIM, 2).astype(jnp.float32) / HEAD_DIM)
    angles = positions[:, None] * freqs[None, :]
    att_query = rotate((proj_qa * inverse).reshape(tok_rows, att_local, HEAD_DIM), angles).astype(
        jnp.bfloat16
    )
    att_key = rotate((proj_ka * inverse).reshape(tok_rows, nearby_memory, HEAD_DIM), angles).astype(
        jnp.bfloat16
    )
    att_value = (proj_va * inverse).astype(jnp.bfloat16).reshape(tok_rows, nearby_memory, HEAD_DIM)
    stacked = jnp.stack([att_key, att_value])
    widened_pair = with_halo(stacked, (("sp", 1),), SPAN_RADIUS)
    block_rows = min(tok_rows, 512)
    sink_logit = sink.reshape(nearby_memory, group)
    grouped_query = att_query.reshape(tok_rows, nearby_memory, group, HEAD_DIM)

    def attend_block(index):
        begin = index * block_rows
        block_keys = widened_pair[0]
        block_values = widened_pair[1]
        scores = jnp.einsum(
            "qhgd,khd->hgqk", grouped_query, block_keys, preferred_element_type=jnp.float32
        ) * HEAD_DIM ** (-0.5)
        query_pos = offset + begin + jnp.arange(block_rows, dtype=jnp.int32)
        key_pos = (
            offset + begin - SPAN_RADIUS + jnp.arange(block_rows + 2 * SPAN_RADIUS, dtype=jnp.int32)
        )
        spacing = key_pos[None, :] - query_pos[:, None]
        valid = (
            (jnp.abs(spacing) <= SPAN_RADIUS)
            & (key_pos >= 0)[None, :]
            & (key_pos < total_rows)[None, :]
        )
        masked = jnp.where(valid, scores, -jnp.inf)
        top = jnp.maximum(jnp.max(masked, axis=-1), sink_logit[:, :, None])
        expo = jnp.exp(masked - top[..., None])
        total = jnp.sum(expo, axis=-1) + jnp.exp(sink_logit[:, :, None] - top)
        logs = top + jnp.log(total)
        probs = (expo / total[..., None]).astype(jnp.bfloat16)
        result = jnp.einsum(
            "hgqk,khd->qhgd", probs, block_values, preferred_element_type=jnp.float32
        ).astype(jnp.bfloat16)
        return (
            result.reshape(block_rows, att_local * HEAD_DIM),
            logs.reshape(att_local, block_rows),
        )

    att_blocks, log_blocks = lax.map(
        attend_block, jnp.arange(tok_rows // block_rows, dtype=jnp.int32)
    )
    att_out = att_blocks.reshape(tok_rows, att_local * HEAD_DIM)
    log_weight = jnp.moveaxis(log_blocks, 0, 1).reshape(att_local, tok_rows)
    ret_query = (proj_qr * inverse).astype(jnp.bfloat16).reshape(tok_rows, ret_local, HEAD_DIM)
    ret_key = (
        (proj_kr * (inverse * HEAD_DIM ** (-0.5)))
        .astype(jnp.bfloat16)
        .reshape(tok_rows, ret_local, HEAD_DIM)
    )
    ret_value = (proj_vr * inverse).astype(jnp.bfloat16).reshape(tok_rows, ret_local, HEAD_DIM)
    cumul = jnp.cumsum(decay_log, axis=1)
    last = cumul[:, -1]
    query_f = ret_query.astype(jnp.float32)
    key_f = ret_key.astype(jnp.float32)
    value_f = ret_value.astype(jnp.float32)
    ret_scores = jnp.einsum("qhd,khd->hqk", ret_query, ret_key, preferred_element_type=jnp.float32)
    decay_weights = jnp.exp(-jnp.abs(cumul[:, :, None] - cumul[:, None, :]))
    inner = jnp.einsum("hqk,khd->qhd", ret_scores * decay_weights, value_f, precision=highest)
    trailing = jnp.exp(last[:, None] - cumul)
    leading = jnp.exp(cumul)
    forward_state = jnp.einsum("hk,khd,khe->hde", trailing, key_f, value_f, precision=highest)
    backward_state = jnp.einsum("hk,khd,khe->hde", leading, key_f, value_f, precision=highest)
    decay_total = jnp.exp(last)
    identity = (jnp.ones_like(decay_total), jnp.zeros_like(forward_state))
    from_before = entering((decay_total, forward_state), "sp", chain, identity, False)[1]
    from_after = entering((decay_total, backward_state), "sp", chain, identity, True)[1]
    carried = leading.T[:, :, None] * jnp.einsum(
        "qhd,hde->qhe", query_f, from_before, precision=highest
    )
    carried = carried + trailing.T[:, :, None] * jnp.einsum(
        "qhd,hde->qhe", query_f, from_after, precision=highest
    )
    blended_output = inner + carried
    middle_point = blended_output - jnp.mean(blended_output, axis=-1, keepdims=True)
    normed = middle_point * lax.rsqrt(
        jnp.mean(middle_point * middle_point, axis=-1, keepdims=True) + 1e-06
    )
    ret_out = normed.astype(jnp.bfloat16).reshape(tok_rows, ret_local * HEAD_DIM)
    wide_out_att, wide_out_ret = (
        lax.all_gather(out_att, "sp", axis=1, tiled=True),
        lax.all_gather(out_ret, "sp", axis=1, tiled=True),
    )
    mixed = lax.psum_scatter(
        (
            jnp.dot(att_out, wide_out_att, preferred_element_type=jnp.float32)
            + jnp.dot(ret_out, wide_out_ret, preferred_element_type=jnp.float32)
        ).astype(jnp.bfloat16),
        "tp",
        scatter_dimension=0,
        tiled=True,
    )
    return (mixed, log_weight)


def solution(mesh):
    return jax.shard_map(
        shards,
        mesh=mesh,
        in_specs=(
            P("sp", "tp"),
            P("tp"),
            P("sp", "tp"),
            P("sp", "tp"),
            P("sp", "tp"),
            P("sp", "tp"),
            P("sp", "tp"),
            P("sp", "tp"),
            P("tp", "sp"),
            P("tp", "sp"),
            P("tp"),
            P("tp", "sp"),
        ),
        out_specs=(P(("sp", "tp"), None), P("tp", "sp")),
        check_vma=False,
    )
```

profile of v0, /device:TPU:0, one launch (start us, length us, event | category | flops | bytes accessed | tf_op | source)
XLA Modules:
  0.0 895.8 jit_solution(7735527587921231865)
XLA Ops:
  7.2 2.5 fusion.6
  13.0 1.2 reduce-window.6
  14.8 2.6 psum.7
  17.5 5.9 all-gather.15.cloned.1.call-done
  23.4 79.6 %all-gather.29.cloned.1.call-done = bf16[4096,512]{1,0:T(8,128)(2,1)} async-done(((bf16[256,512]{1,0:T(8,128)(2,1)}), bf16[4096,512]{1,0:T(8,128)(2,1)}) %all-gather.29.cloned.1.call-update) | async-done | bytes 4194320 | tf_op jit(solution)/shard_map/all_gather | solution.py:87
  103.0 4.1 fusion.17
  107.2 72.8 %all-gather.25.cloned.1.call-done = bf16[4096,512]{1,0:T(8,128)(2,1)} async-done(((bf16[256,512]{1,0:T(8,128)(2,1)}), bf16[4096,512]{1,0:T(8,128)(2,1)}) %all-gather.25.cloned.1.call-update) | async-done | bytes 4194320 | tf_op jit(solution)/shard_map/all_gather | solution.py:88
  180.0 4.1 fusion.19
  184.1 1.1 convolution_convert_fusion
  185.3 1.0 convolution_convert_fusion.1
  190.1 39.8 %all-reduce = bf16[64]{0:T(256)(128)(2,1)S(1)} all-reduce(bf16[64]{0:T(256)(128)(2,1)S(1)} %dynamic-update-slice), channel_id=2, replica_groups=mesh['sp'=16,'tp'=2] {'sp'}, use_global_device_ids=true, to_apply=%add | all-reduce | flops 64 | bytes 256
  231.4 25.6 %all-gather.17.cloned.1.call-done = bf16[4096,512]{1,0:T(8,128)(2,1)} async-done(((bf16[256,512]{1,0:T(8,128)(2,1)}), bf16[4096,512]{1,0:T(8,128)(2,1)}) %all-gather.17.cloned.1.call-update) | async-done | bytes 4194320 | tf_op jit(solution)/shard_map/all_gather | solution.py:84
  257.1 4.1 convolution_multiply_fusion.6
  261.7 72.2 %all-gather.19.cloned.1.call-done = bf16[4096,512]{1,0:T(8,128)(2,1)} async-done(((bf16[256,512]{1,0:T(8,128)(2,1)}), bf16[4096,512]{1,0:T(8,128)(2,1)}) %all-gather.19.cloned.1.call-update) | async-done | bytes 4194320 | tf_op jit(solution)/shard_map/all_gather | solution.py:85
  333.9 4.1 fusion.14
  339.2 3.4 collective-permute-start
  342.6 1.3 collective-permute-start.1
  343.9 70.2 %all-gather.27.cloned.1.call-done = bf16[4096,512]{1,0:T(8,128)(2,1)} async-done(((bf16[256,512]{1,0:T(8,128)(2,1)}), bf16[4096,512]{1,0:T(8,128)(2,1)}) %all-gather.27.cloned.1.call-update) | async-done | bytes 4194320 | tf_op jit(solution)/shard_map/all_gather | solution.py:86
  414.0 4.1 fusion.18
  418.2 1.3 convolution_multiply_fusion
  419.4 1.1 pad_maximum_fusion
  420.6 55.2 %all-gather.35.cloned.1.call-done = bf16[64,128,128]{2,1,0:T(8,128)(2,1)} async-done(((bf16[4,128,128]{2,1,0:T(8,128)(2,1)}), bf16[64,128,128]{2,1,0:T(8,128)(2,1)}) %all-gather.35.cloned.1.call-update) | async-done | bytes 2097168 | tf_op jit(solution)/shard_map/all_gather | solution.py:27
  475.8 27.7 %while.36 = (s32[]{:T(128)}, f32[4,128,128]{2,1,0:T(8,128)S(1)}, s32[]{:T(128)}, bf16[16,4]{1,0:T(8,128)(2,1)}, bf16[16,4,128,128]{3,2,1,0:T(8,128)(2,1)}, /*index=5*/s32[]{:T(128)}, s32[]{:T(128)}, s32[]{:T(128)}, s32[]{:T(128)}) while((s32[]{:T(128)}, f32[4,128,128]{2,1,0:T(8,128)S(1)}, s32[]{:T(128)}, bf16[16,4]{1,0:T(8,128)(2,1)}, ...), condition=%wide.region_9.10_spmd.clone, body=%wide.region_8.9_spmd.clone.sunk | while | flops 327692 | bytes 655567 | solution.py:45
  476.6 1.0 fusion.75
  478.3 1.0 fusion.75
  480.0 1.0 fusion.75
  481.8 1.0 fusion.75
  483.5 1.0 fusion.75
  485.2 1.0 fusion.75
  486.9 1.0 fusion.75
  488.7 1.0 fusion.75
  490.4 1.0 fusion.75
  492.1 1.0 fusion.75
  493.8 1.0 fusion.75
  495.6 1.0 fusion.75
  497.3 1.0 fusion.75
  499.0 1.0 fusion.75
  500.7 1.0 fusion.75
  502.5 1.0 fusion.75
  503.5 34.4 %all-gather.33.cloned.1.call-done = bf16[64,128,128]{2,1,0:T(8,128)(2,1)} async-done(((bf16[4,128,128]{2,1,0:T(8,128)(2,1)}), bf16[64,128,128]{2,1,0:T(8,128)(2,1)}) %all-gather.33.cloned.1.call-update) | async-done | bytes 2097168 | tf_op jit(solution)/shard_map/all_gather | solution.py:27
  537.9 27.5 %while.35 = (s32[]{:T(128)}, f32[4,128,128]{2,1,0:T(8,128)S(1)}, s32[]{:T(128)}, bf16[16,4]{1,0:T(8,128)(2,1)}, bf16[16,4,128,128]{3,2,1,0:T(8,128)(2,1)}, /*index=5*/s32[]{:T(128)}, s32[]{:T(128)}) while((s32[]{:T(128)}, f32[4,128,128]{2,1,0:T(8,128)S(1)}, s32[]{:T(128)}, bf16[16,4]{1,0:T(8,128)(2,1)}, ...), condition=%wide.region_7.8_spmd.clone, body=%wide.region_6.7_spmd.clone.sunk | while | flops 327688 | bytes 655505 | solution.py:45
  538.6 1.0 fusion.74
  540.3 1.0 fusion.74
  542.0 1.0 fusion.74
  547.2 1.0 fusion.74
  548.9 1.0 fusion.74
  550.6 1.0 fusion.74
  552.4 1.0 fusion.74
  554.1 1.0 fusion.74
  555.8 1.0 fusion.74
  557.5 1.0 fusion.74
  559.2 1.0 fusion.74
  560.9 1.0 fusion.74
  562.7 1.0 fusion.74
  564.4 1.0 fusion.74
  567.2 84.6 %all-gather.21.cloned.1.call-done = bf16[4096,1024]{1,0:T(8,128)(2,1)} async-done(((bf16[256,1024]{1,0:T(8,128)(2,1)}), bf16[4096,1024]{1,0:T(8,128)(2,1)}) %all-gather.21.cloned.1.call-update) | async-done | bytes 8388624 | tf_op jit(solution)/shard_map/all_gather | solution.py:83
  651.8 6.3 fusion.8
  659.0 1.0 fusion.4
  661.1 1.3 fusion.9
  662.4 124.7 %all-gather.23.cloned.1.call-done = bf16[1024,4096]{1,0:T(8,128)(2,1)} async-done(((bf16[1024,256]{1,0:T(8,128)(2,1)}), bf16[1024,4096]{1,0:T(8,128)(2,1)}) %all-gather.23.cloned.1.call-update) | async-done | bytes 8388624 | tf_op jit(solution)/shard_map/all_gather | solution.py:182
  787.1 7.8 fusion.51
  794.8 80.0 %all-gather.31.cloned.1.call-done = bf16[512,4096]{1,0:T(8,128)(2,1)} async-done(((bf16[512,256]{1,0:T(8,128)(2,1)}), bf16[512,4096]{1,0:T(8,128)(2,1)}) %all-gather.31.cloned.1.call-update) | async-done | bytes 4194320 | tf_op jit(solution)/shard_map/all_gather | solution.py:183
  874.8 6.1 fusion.2
  881.6 7.4 reduce-scatter.2.cloned.1.call-done
  (130 shorter events, 38.9 us)
Async XLA Ops:
  7.2 5.9 copy-start.3
  7.2 16.3 %all-gather.15.cloned.1.call-start = ((), (), s32[]{:S(2)}) async-start(), calls=%async_computation.1 | async-start | bytes 3145728 | tf_op jit(solution)/shard_map/all_gather | solution.py:92
  9.7 93.3 %all-gather.29.cloned.1.call-start = ((), (), s32[]{:S(2)}) async-start(), calls=%async_computation.8 | async-start | bytes 4456448 | tf_op jit(solution)/shard_map/all_gather | solution.py:87
  10.5 169.5 %all-gather.25.cloned.1.call-start = ((), (), s32[]{:S(2)}) async-start(), calls=%async_computation.6 | async-start | bytes 4456448 | tf_op jit(solution)/shard_map/all_gather | solution.py:88
  11.2 245.8 %all-gather.17.cloned.1.call-start = ((), (), s32[]{:S(2)}) async-start(), calls=%async_computation.2 | async-start | bytes 4456448 | tf_op jit(solution)/shard_map/all_gather | solution.py:84
  11.8 322.1 %all-gather.19.cloned.1.call-start = ((), (), s32[]{:S(2)}) async-start(), calls=%async_computation.3 | async-start | bytes 4456448 | tf_op jit(solution)/shard_map/all_gather | solution.py:85
  12.4 401.6 %all-gather.27.cloned.1.call-start = ((), (), s32[]{:S(2)}) async-start(), calls=%async_computation.7 | async-start | bytes 4456448 | tf_op jit(solution)/shard_map/all_gather | solution.py:86
  13.0 462.8 %all-gather.35.cloned.1.call-start = ((), (), s32[]{:S(2)}) async-start(), calls=%async_computation.12 | async-start | bytes 2228224 | tf_op jit(solution)/shard_map/all_gather | solution.py:27
  17.5 316.5 %copy-start.6 = (f32[256]{0:T(256)}, f32[256]{0:T(256)S(1)}, u32[]{:S(2)}) copy-start(f32[256]{0:T(256)S(1)} %get-tuple-element.322) | copy-start | bytes 3076
  107.2 78.0 %copy-start.1 = (bf16[256,512]{0,1:T(8,128)(2,1)}, bf16[256,512]{0,1:T(8,128)(2,1)S(1)}, u32[]{:S(2)}) copy-start(bf16[256,512]{0,1:T(8,128)(2,1)S(1)} %copy.80) | copy-start | bytes 786436
  180.0 8.5 copy-start.4
  180.0 8.6 copy-start.8
  185.2 352.7 %all-gather.33.cloned.1.call-start = ((), (), s32[]{:S(2)}) async-start(), calls=%async_computation.11 | async-start | bytes 2228224 | tf_op jit(solution)/shard_map/all_gather | solution.py:27
  186.3 465.5 %all-gather.21.cloned.1.call-start = ((), (), s32[]{:S(2)}) async-start(), calls=%async_computation.4 | async-start | bytes 8912896 | tf_op jit(solution)/shard_map/all_gather | solution.py:83
  187.1 600.0 %all-gather.23.cloned.1.call-start = ((), (), s32[]{:S(2)}) async-start(), calls=%async_computation.5 | async-start | bytes 8912896 | tf_op jit(solution)/shard_map/all_gather | solution.py:182
  187.6 687.1 %all-gather.31.cloned.1.call-start = ((), (), s32[]{:S(2)}) async-start(), calls=%async_computation.9 | async-start | bytes 4456448 | tf_op jit(solution)/shard_map/all_gather | solution.py:183
  188.4 700.6 %reduce-scatter.2.cloned.1.call-start = ((), (), s32[]{:S(2)}) async-start(), calls=%async_computation.10 | async-start | bytes 3145728 | tf_op jit(solution)/shard_map/reduce_scatter | solution.py:185
  338.4 79.7 %copy-start.2 = (bf16[256,512]{0,1:T(8,128)(2,1)S(1)}, bf16[256,512]{0,1:T(8,128)(2,1)}, u32[]{:S(2)}) copy-start(bf16[256,512]{0,1:T(8,128)(2,1)} %copy-done.1) | copy-start | bytes 786436
  339.2 80.2 %collective-permute-start = (bf16[2,128,4,128]{3,1,2,0:T(8,128)(2,1)}, bf16[2,128,4,128]{3,1,2,0:T(8,128)(2,1)S(1)}, u32[]{:S(2)}, u32[]{:S(2)}) collective-permute-start(bf16[2,128,4,128]{3,1,2,0:T(8,128)(2,1)} %get-tuple-element.313), channel_id=1, source_target_pairs={{0,2},{2,4},{4,6},{6,8},{8,10},{10,12},{12,14},{14,16},{16,18},{18... | collective-permute-start | bytes 786440 | tf_op jit(solution)/shard_map/ppermute | solution.py:18
  342.6 76.9 %collective-permute-start.1 = (bf16[2,128,4,128]{3,1,2,0:T(8,128)(2,1)S(1)}, bf16[2,128,4,128]{3,1,2,0:T(8,128)(2,1)}, u32[]{:S(2)}, u32[]{:S(2)}) collective-permute-start(bf16[2,128,4,128]{3,1,2,0:T(8,128)(2,1)S(1)} %get-tuple-element.314), channel_id=1, source_target_pairs={{2,0},{4,2},{6,4},{8,6},{10,8},{12,10},{14,12},{16,14},{18,16},{20... | collective-permute-start | bytes 786440 | tf_op jit(solution)/shard_map/ppermute | solution.py:19
  475.8 90.5 %copy-start = (f32[4,256,256]{2,1,0:T(8,128)S(1)}, f32[4,256,256]{2,1,0:T(8,128)}, u32[]{:S(2)}) copy-start(f32[4,256,256]{2,1,0:T(8,128)} %convolution_multiply_fusion) | copy-start | bytes 3145732
  565.4 86.4 %copy-start.7 = (f32[256]{0:T(256)S(1)}, f32[256]{0:T(256)}, u32[]{:S(2)}) copy-start(f32[256]{0:T(256)} %copy-done.6) | copy-start | bytes 3076
  874.8 6.1 copy-start.5
Sparse Core Ops, SparseCore 0:
  10.1 13.2 all-gather.14
  26.2 76.7 all-gather.28
  105.8 74.1 all-gather.24
  182.6 74.4 all-gather.16
  259.7 74.1 all-gather.18
  336.5 77.4 all-gather.26
  416.8 58.9 all-gather.34
  478.6 59.2 all-gather.32
  540.7 111.0 all-gather.20
  654.4 132.6 all-gather.22
  789.8 84.9 all-gather.30
  881.0 7.9 reduce-scatter.1
where the time goes:
time: 897 us; the launch traced here: 896 us
  waiting for transfers between devices  717 us (80%)
  other arithmetic  63.1 us (7%)
  matrix products  47.8 us (5%)
  blocking collectives  42.4 us (5%)
  between operations  15.3 us (2%)
    all_gather x1, waiting for transfers between devices, shards(): lax.all_gather(out_att, 'sp', axis=1, tiled=True)  125 us
    all_gather x2, waiting for transfers between devices, entering(): lax.all_gather(part.astype(kind), axis)  89.6 us
    all_gather x1, waiting for transfers between devices, shards(): lax.all_gather(q_att, 'sp', axis=0, tiled=True)  84.6 us
    all_gather x1, waiting for transfers between devices, shards(): lax.all_gather(out_ret, 'sp', axis=1, tiled=True)  80 us
    all_gather x1, waiting for transfers between devices, shards(): lax.all_gather(k_ret, 'sp', axis=0, tiled=True)  79.6 us
    all_gather x1, waiting for transfers between devices, shards(): lax.all_gather(v_ret, 'sp', axis=0, tiled=True)  72.8 us
    all_gather x1, waiting for transfers between devices, shards(): lax.all_gather(v_att, 'sp', axis=0, tiled=True)  72.2 us
    all_gather x1, waiting for transfers between devices, shards(): lax.all_gather(q_ret, 'sp', axis=0, tiled=True)  70.2 us
  transfers between devices with their start and end apart: 14, of which 12 were waited for; matrix products, arithmetic and copies ran while one was open for 12% of the time, Pallas kernels for 0%

commit v1 on v0

v1 whole, which is shorter than its diff:
```python
import math

import jax
import jax.numpy as jnp
from jax import lax
from jax.sharding import Mesh
from jax.sharding import PartitionSpec as P

HEAD_DIM = 128
SPAN_RADIUS = 128
BLOCK = 256
HIGHEST = lax.Precision.HIGHEST


def gather(x, axis, dim):
    if lax.axis_size(axis) == 1:
        return x
    return lax.all_gather(x, axis, axis=dim, tiled=True)


def exchange(x, axis, split, concat):
    if lax.axis_size(axis) == 1:
        return x
    return lax.all_to_all(x, axis, split, concat, tiled=True)


def halo(shard, axis, width):
    peers, length = lax.axis_size(axis), shard.shape[1]
    up = [(i, i + 1) for i in range(peers - 1)]
    down = [(j, i) for i, j in up]
    before = lax.ppermute(shard[:, length - width :], axis, up)
    after = lax.ppermute(shard[:, :width], axis, down)
    return jnp.concatenate([before, shard, after], axis=1)


def rotate(values, cosine, sine):
    half = values.shape[-1] // 2
    first, second = values[..., :half], values[..., half:]
    return jnp.concatenate(
        [first * cosine - second * sine, second * cosine + first * sine], axis=-1
    ).astype(jnp.bfloat16)


def attend(query, key, value, sink, offset, total_rows):
    rows, kv, group, _ = query.shape
    ext = halo(jnp.stack([key, value]), "t", SPAN_RADIUS)
    size = min(rows, BLOCK)
    count = rows // size
    span = size + 2 * SPAN_RADIUS
    pieces = jnp.stack([ext[:, b * size : b * size + span] for b in range(count)])
    blocks = query.reshape(count, size, kv, group, HEAD_DIM)
    scores = jnp.einsum(
        "bqhgd,bkhd->bhgqk", blocks, pieces[:, 0], preferred_element_type=jnp.float32
    ) * HEAD_DIM ** (-0.5)
    base = offset + jnp.arange(count, dtype=jnp.int32) * size
    query_pos = base[:, None] + jnp.arange(size, dtype=jnp.int32)
    key_pos = base[:, None] - SPAN_RADIUS + jnp.arange(span, dtype=jnp.int32)
    spacing = key_pos[:, None, :] - query_pos[:, :, None]
    inside = (key_pos >= 0) & (key_pos < total_rows)
    valid = (jnp.abs(spacing) <= SPAN_RADIUS) & inside[:, None, :]
    masked = jnp.where(valid[:, None, None], scores, -jnp.inf)
    limit = sink[None, :, :, None]
    top = jnp.maximum(jnp.max(masked, axis=-1), limit)
    expo = jnp.exp(masked - top[..., None])
    total = jnp.sum(expo, axis=-1) + jnp.exp(limit - top)
    logs = top + jnp.log(total)
    probs = (expo / total[..., None]).astype(jnp.bfloat16)
    result = jnp.einsum(
        "bhgqk,bkhd->bqhgd", probs, pieces[:, 1], preferred_element_type=jnp.float32
    ).astype(jnp.bfloat16)
    logs = jnp.transpose(logs, (1, 2, 0, 3)).reshape(kv * group, rows)
    return result.reshape(rows, kv * group * HEAD_DIM), logs


def retain(query, key, value, decay):
    rows, heads, _ = query.shape
    peers, index = lax.axis_size("t"), lax.axis_index("t")
    cumul = jnp.cumsum(decay, axis=1)
    last = cumul[:, -1]
    query_f, key_f, value_f = (v.astype(jnp.float32) for v in (query, key, value))
    trailing = jnp.exp(last[:, None] - cumul)
    leading = jnp.exp(cumul)
    forward = jnp.einsum("hk,khd,khe->hde", trailing, key_f, value_f, precision=HIGHEST)
    backward = jnp.einsum("hk,khd,khe->hde", leading, key_f, value_f, precision=HIGHEST)
    tail = jnp.broadcast_to(last[:, None, None], (heads, 8, HEAD_DIM))
    sent = jnp.concatenate([forward, backward, tail], axis=1)
    seen = lax.all_gather(sent, "t", axis=0)
    lasts = seen[:, :, 2 * HEAD_DIM, 0]
    at = jnp.arange(peers)
    low = jnp.minimum(at, index)[:, None]
    high = jnp.maximum(at, index)[:, None]
    between = (at[None, :] > low) & (at[None, :] < high)
    spans = jnp.exp(jnp.sum(jnp.where(between[:, :, None], lasts[None], 0.0), axis=1))
    before = jnp.sum(
        jnp.where(at < index, 1.0, 0.0)[:, None, None, None]
        * spans[:, :, None, None]
        * seen[:, :, :HEAD_DIM],
        axis=0,
    )
    after = jnp.sum(
        jnp.where(at > index, 1.0, 0.0)[:, None, None, None]
        * spans[:, :, None, None]
        * seen[:, :, HEAD_DIM : 2 * HEAD_DIM],
        axis=0,
    )
    scores = jnp.einsum("qhd,khd->hqk", query, key, preferred_element_type=jnp.float32)
    weights = jnp.exp(-jnp.abs(cumul[:, :, None] - cumul[:, None, :]))
    mix = jnp.einsum("hqk,khd->qhd", scores * weights, value_f, precision=HIGHEST)
    mix = mix + leading.T[:, :, None] * jnp.einsum(
        "qhd,hde->qhe", query_f, before, precision=HIGHEST
    )
    mix = mix + trailing.T[:, :, None] * jnp.einsum(
        "qhd,hde->qhe", query_f, after, precision=HIGHEST
    )
    middle = mix - jnp.mean(mix, axis=-1, keepdims=True)
    normed = middle * lax.rsqrt(jnp.mean(middle * middle, axis=-1, keepdims=True) + 1e-06)
    return normed.astype(jnp.bfloat16).reshape(rows, heads * HEAD_DIM)


def shards(
    tokens, gain, q_att, k_att, v_att, q_ret, k_ret, v_ret, out_att, out_ret, sink, decay_log
):
    parts = lax.axis_size("h")
    own = tokens.shape[0]
    rows = own * parts
    width = tokens.shape[1] * lax.axis_size("tp")
    kv = k_att.shape[1] // HEAD_DIM // parts
    group = q_att.shape[1] // k_att.shape[1]
    att = kv * group
    ret = q_ret.shape[1] // HEAD_DIM // parts
    offset = lax.axis_index("t") * rows
    total_rows = rows * lax.axis_size("t")

    packed = jnp.concatenate(
        [
            w.reshape(w.shape[0], parts, w.shape[1] // parts)
            for w in (q_att, k_att, v_att, q_ret, k_ret, v_ret)
        ],
        axis=2,
    )
    packed = jnp.moveaxis(packed, 1, 0).reshape(parts * packed.shape[0], packed.shape[2])
    weight = gather(exchange(packed, "h", 0, 0), "t", 0)

    widened = tokens.astype(jnp.float32)
    sums = lax.all_gather(jnp.sum(widened * widened, axis=1), ("h", "tp"))
    squares = jnp.sum(sums.reshape(parts, lax.axis_size("tp"), own), axis=1).reshape(rows)
    inverse = lax.rsqrt(squares / width + 1e-06)[:, None]
    scaled = (widened * gain).astype(jnp.bfloat16)
    whole = gather(gather(scaled, "h", 0), "tp", 1)
    proj = jnp.dot(whole, weight, preferred_element_type=jnp.float32)

    edges = [att, kv, kv, ret, ret, ret]
    starts = [sum(edges[:i]) * HEAD_DIM for i in range(6)]
    qa, ka, va, qr, kr, vr = (
        proj[:, s : s + n * HEAD_DIM].reshape(rows, n, HEAD_DIM) for s, n in zip(starts, edges)
    )
    scale = inverse[:, :, None]
    positions = (offset + jnp.arange(rows, dtype=jnp.int32)).astype(jnp.float32)
    freqs = 10000.0 ** (-jnp.arange(0, HEAD_DIM, 2).astype(jnp.float32) / HEAD_DIM)
    angles = positions[:, None] * freqs[None, :]
    cosine, sine = jnp.cos(angles)[:, None, :], jnp.sin(angles)[:, None, :]
    att_query = rotate(qa * scale, cosine, sine)
    att_key = rotate(ka * scale, cosine, sine)
    att_value = (va * scale).astype(jnp.bfloat16)
    ret_query = (qr * scale).astype(jnp.bfloat16)
    ret_key = (kr * (scale * HEAD_DIM ** (-0.5))).astype(jnp.bfloat16)
    ret_value = (vr * scale).astype(jnp.bfloat16)

    logits = lax.dynamic_slice_in_dim(sink, lax.axis_index("h") * att, att).reshape(kv, group)
    att_out, logs = attend(
        att_query.reshape(rows, kv, group, HEAD_DIM), att_key, att_value, logits, offset, total_rows
    )
    ret_out = retain(ret_query, ret_key, ret_value, exchange(decay_log, "h", 0, 1))

    out_pack = jnp.concatenate(
        [w.reshape(parts, w.shape[0] // parts, w.shape[1]) for w in (out_att, out_ret)], axis=1
    )
    out_wide = gather(exchange(out_pack, "h", 0, 0), "t", 0)
    depth = out_wide.shape[1]
    out_wide = jnp.moveaxis(out_wide, 0, 1).reshape(depth, -1)
    mixed = jnp.dot(
        jnp.concatenate([att_out, ret_out], axis=1), out_wide, preferred_element_type=jnp.float32
    ).astype(jnp.bfloat16)
    mixed = lax.psum_scatter(mixed, ("h", "tp"), scatter_dimension=0, tiled=True)
    return mixed, exchange(logs, "h", 1, 0)


def solution(mesh):
    sp, tp = mesh.shape["sp"], mesh.shape["tp"]

    def run(*args):
        heads = math.gcd(args[3].shape[1], args[5].shape[1]) // HEAD_DIM
        parts = math.gcd(heads // math.gcd(heads, tp), sp)
        fine = Mesh(mesh.devices.reshape(sp // parts, parts, tp), ("t", "h", "tp"))
        seq = ("t", "h")
        body = jax.shard_map(
            shards,
            mesh=fine,
            in_specs=(P(seq, "tp"), P("tp"))
            + (P(seq, "tp"),) * 6
            + (P("tp", seq), P("tp", seq), P("tp"), P("tp", seq)),
            out_specs=(P(("t", "h", "tp"), None), P("tp", seq)),
            check_vma=False,
        )
        return body(*args)

    return run
```

time: 897 us -> 440 us (0.49)
  waiting for transfers between devices: 717 us -> 270 us
  other arithmetic: 63.1 us -> 12 us
  blocking collectives: 42.4 us -> 89 us
  matrix products: 47.8 us -> 28.2 us
  local copies, waits for them, and re-layouts: 4 us -> 16.1 us
    all_gather x11 -> x4, waiting for transfers between devices: 705 us -> 205 us  [gather(): return lax.all_gather(x, axis, axis=dim, tiled=True)]
    all_to_all x0 -> x3, blocking collectives: none -> 62.6 us  [exchange(): return lax.all_to_all(x, axis, split, concat, tiled=True)]
    reduce_scatter x1, waiting for transfers between devices: 7.37 us -> 64.5 us  [shards(): lax.psum_scatter(mixed, ('h', 'tp'), scatter_dimension=0, tiled=True)]
    unnamed x1 -> x0, blocking collectives: 39.8 us -> none
    select_n x32 -> x0, other arithmetic: 32.3 us -> none  [turn(): return jax.tree.map(lambda a, b: jnp.where(reached, a, b), new, before)]
    all_gather x0 -> x2, blocking collectives: none -> 26.4 us  [the longest x1 17.1 us: retain(): seen = lax.all_gather(sent, 't', axis=0)]
    convert_element_type x34 -> x1, other arithmetic: 22.3 us -> 0.01 us  [shards(): positions = (offset + jnp.arange(rows, dtype=jnp.int32)).astype(jnp.float32)]
    dot_general x16 -> x10, matrix products: 47.8 us -> 28.2 us  [the longest x1 11.4 us: shards(): proj = jnp.dot(whole, weight, preferred_element_type=jnp.float32)]
  transfers between devices with their start and end apart: 14 -> 8, of which waited for: 12 -> 5; matrix products, arithmetic and copies ran while one was open for 12% -> 5% of each run, Pallas kernels for 0% -> 0%
where the time goes in v1:
time: 440 us
  waiting for transfers between devices  270 us (61%)
  blocking collectives  89 us (20%)
  matrix products  28.2 us (6%)
  local copies, waits for them, and re-layouts  16.1 us (4%)
  between operations  15.6 us (4%)
  other arithmetic  12 us (3%)
  starting transfers between devices  9.02 us (2%)
    all_gather x4, waiting for transfers between devices, gather(): return lax.all_gather(x, axis, axis=dim, tiled=True)  205 us
    reduce_scatter x1, waiting for transfers between devices, shards(): lax.psum_scatter(mixed, ('h', 'tp'), scatter_dimension=0, tiled=True)  64.5 us
    all_to_all x3, blocking collectives, exchange(): return lax.all_to_all(x, axis, split, concat, tiled=True)  62.6 us
    all_gather x1, blocking collectives, retain(): seen = lax.all_gather(sent, 't', axis=0)  17.1 us
    dot_general x1, matrix products, shards(): proj = jnp.dot(whole, weight, preferred_element_type=jnp.float32)  11.4 us
    all_gather x1, blocking collectives, shards(): sums = lax.all_gather(jnp.sum(widened * widened, axis=1), ('h', 'tp'))  9.34 us
  transfers between devices with their start and end apart: 8, of which 5 were waited for; matrix products, arithmetic and copies ran while one was open for 5% of the time, Pallas kernels for 0%

profile of v1, /device:TPU:0, one launch (start us, length us, event | category | flops | bytes accessed | tf_op | source)
XLA Modules:
  0.0 439.8 jit_solution(1814803313138808703)
XLA Ops:
  7.3 2.6 fusion.9
  9.9 1.2 pad_maximum_fusion.1
  11.1 20.5 %all_to_all.46 = bf16[4,384,256]{2,1,0:T(8,128)(2,1)} all-to-all(bf16[4,384,256]{2,1,0:T(8,128)(2,1)S(1)} %pad_maximum_fusion.1), channel_id=1, replica_groups=mesh['t'=4,'h'=4,'tp'=2] {'h'}, dimensions={0} | all-to-all | bytes 1572864 | tf_op jit(solution)/shard_map/all_to_all | solution.py:24
  31.7 0.2 copy.67
  32.0 0.1 copy.68
  32.1 0.1 copy.69
  32.3 0.1 copy.70
  32.4 0.1 copy.71
  32.6 0.1 copy.72
  32.9 34.0 %all_to_all.47 = bf16[4,256,896]{1,2,0:T(8,128)(2,1)S(1)} all-to-all(bf16[4,256,896]{1,2,0:T(8,128)(2,1)S(1)} %bitcast.161), channel_id=1, replica_groups=mesh['t'=4,'h'=4,'tp'=2] {'h'}, dimensions={0} | all-to-all | bytes 3670016 | tf_op jit(solution)/shard_map/all_to_all | solution.py:24
  66.8 2.4 copy.73
  69.3 11.3 %all-gather.8.cloned.1.call-done = bf16[1024,2048]{1,0:T(8,128)(2,1)} async-done(((bf16[256,2048]{1,0:T(8,128)(2,1)}), bf16[1024,2048]{1,0:T(8,128)(2,1)}) %all-gather.8.cloned.1.call-update) | async-done | bytes 4194320 | tf_op jit(solution)/shard_map/all_gather | solution.py:18
  80.6 0.6 all_to_all.35
  81.2 3.2 all-to-all-start.1
  84.5 9.3 %all-gather.2 = f32[8,1,256]{2,1,0:T(1,128)S(1)} all-gather(f32[1,1,256]{2,1,0:T(1,128)S(1)} %bitcast.180), channel_id=2, replica_groups=mesh['t'=4,'h'=4,'tp'=2] {'h','tp'}, dimensions={0}, use_global_device_ids=true | all-gather | bytes 9216 | tf_op jit(solution)/shard_map/all_gather | solution.py:145
  94.2 1.0 multiply_cosine_fusion
  95.2 0.8 fusion.14
  96.2 0.3 reduce-window.6
  96.4 0.2 slice_reduce_fusion
  96.6 0.2 reduce-window.9
  96.9 0.6 slice.115
  97.5 0.6 slice.114
  99.4 46.5 %all-gather.14.cloned.1.call-done = bf16[16,384,256]{2,1,0:T(8,128)(2,1)} async-done(((bf16[4,384,256]{2,1,0:T(8,128)(2,1)}), bf16[16,384,256]{2,1,0:T(8,128)(2,1)}) %all-gather.14.cloned.1.call-update) | async-done | bytes 3145744 | tf_op jit(solution)/shard_map/all_gather | solution.py:18
  145.9 4.7 %copy.84 = bf16[16,384,256]{1,2,0:T(8,128)(2,1)} copy(bf16[16,384,256]{2,1,0:T(8,128)(2,1)} %all-gather.14.cloned.1.call-done) | data formatting | bytes 6291456 | tf_op jit(solution)/shard_map/all_gather | solution.py:18
  150.6 128.0 %all-gather.12.cloned.1.call-done = bf16[4096,896]{1,0:T(8,128)(2,1)} async-done(((bf16[1024,896]{1,0:T(8,128)(2,1)}), bf16[4096,896]{1,0:T(8,128)(2,1)}) %all-gather.12.cloned.1.call-update) | async-done | bytes 7340048 | tf_op jit(solution)/shard_map/all_gather | solution.py:18
  278.6 19.5 %all-gather.10.cloned.1.call-done = bf16[1024,4096]{1,0:T(8,128)(2,1)} async-done(((bf16[1024,2048]{1,0:T(8,128)(2,1)}), bf16[1024,4096]{1,0:T(8,128)(2,1)}) %all-gather.10.cloned.1.call-update) | async-done | bytes 8388624 | tf_op jit(solution)/shard_map/all_gather | solution.py:18
  298.1 11.4 %fusion.71 = f32[1024,896]{0,1:T(8,128)S(1)} fusion(bf16[1024,4096]{1,0:T(8,128)(2,1)} %all-gather.10.cloned.1.call-done, bf16[4096,896]{1,0:T(8,128)(2,1)} %all-gather.12.cloned.1.call-done), kind=kOutput, calls=%fused_computation.140 | convolution fusion | flops 7516192768 | bytes 19398656 | tf_op jit(solution)/shard_map/dot_general | solution.py:150
  309.5 0.1 slice.108
  309.6 0.4 fusion.37
  309.9 1.2 fusion.58
  311.1 0.1 fusion.69
  311.3 4.3 collective-permute-start
  315.6 1.3 collective-permute-start.1
  316.9 0.1 broadcast_multiply_fusion
  317.0 0.4 convolution_bitcast_fusion.2
  317.4 0.4 convolution_bitcast_fusion.3
  317.8 0.1 maximum_maximum_fusion
  317.9 17.1 %all-gather.1 = f32[4,264,128]{2,1,0:T(8,128)S(1)} all-gather(f32[1,264,128]{2,1,0:T(8,128)S(1)} %maximum_maximum_fusion), channel_id=3, replica_groups=mesh['t'=4,'h'=4,'tp'=2] {'t'}, dimensions={0}, use_global_device_ids=true | all-gather | bytes 675840 | tf_op jit(solution)/shard_map/all_gather | solution.py:87
  335.0 0.1 slice_reduce_fusion.1
  335.1 0.2 select_reduce_fusion
  335.3 0.7 fusion.72
  336.0 0.1 fusion.52
  336.1 0.4 fusion.28
  336.6 3.2 fusion.19
  339.8 0.5 fusion.70
  340.4 0.2 subtract_convert_fusion
  340.6 0.2 concatenate.52
  340.8 0.3 copy.78
  341.1 0.2 concatenate.53
  341.3 0.3 copy.79
  341.6 0.8 copy.83
  342.5 0.9 fusion.54
  343.4 0.9 fusion.53
  344.3 0.1 pad_maximum_fusion
  344.4 1.1 fusion.7
  345.6 1.0 fusion.6
  346.7 3.3 fusion.22
  350.0 2.0 copy.82
  352.0 1.1 copy.94
  353.1 6.8 %convolution_convert_fusion = bf16[1024,4096]{1,0:T(8,128)(2,1)} fusion(bf16[384,4096]{0,1:T(8,128)(2,1)S(1)} %bitcast.160, bf16[1024,128]{1,0:T(8,128)(2,1)S(1)} %copy-done.8, bf16[1024,256]{1,0:T(8,128)(2,1)S(1)} %bitcast.172), kind=kOutput, calls=%fused_computation | convolution fusion | flops 3226992640 | bytes 12320768 | tf_op jit(solution)/shard_map/dot_general | solution.py:181
  359.9 0.1 fusion.61
  360.0 8.1 %all_to_all.48 = f32[2,4,256]{2,0,1:T(2,128)S(1)} all-to-all(f32[2,4,256]{2,0,1:T(2,128)S(1)} %fusion.61), channel_id=1, replica_groups=mesh['t'=4,'h'=4,'tp'=2] {'h'}, dimensions={1} | all-to-all | bytes 16384 | tf_op jit(solution)/shard_map/all_to_all | solution.py:24
  368.1 0.6 all_to_all.41
  368.7 64.5 %reduce-scatter.2.cloned.1.call-done = bf16[128,4096]{1,0:T(8,128)(2,1)} async-done(((bf16[1024,4096]{1,0:T(8,128)(2,1)}), bf16[128,4096]{1,0:T(8,128)(2,1)}) %reduce-scatter.2.cloned.1.call-update) | async-done | bytes 1048592 | tf_op jit(solution)/shard_map/reduce_scatter | solution.py:184
  (70 shorter events, 1.4 us)
Async XLA Ops:
  7.2 24.6 %copy-start.2 = (bf16[256,1024]{1,0:T(8,128)(2,1)S(1)}, bf16[256,1024]{1,0:T(8,128)(2,1)}, u32[]{:S(2)}) copy-start(bf16[256,1024]{1,0:T(8,128)(2,1)} %param.14) | copy-start | bytes 1572868
  7.2 24.8 %copy-start.3 = (bf16[256,512]{1,0:T(8,128)(2,1)S(1)}, bf16[256,512]{1,0:T(8,128)(2,1)}, u32[]{:S(2)}) copy-start(bf16[256,512]{1,0:T(8,128)(2,1)} %param.15) | copy-start | bytes 786436
  7.2 24.9 %copy-start.4 = (bf16[256,512]{1,0:T(8,128)(2,1)S(1)}, bf16[256,512]{1,0:T(8,128)(2,1)}, u32[]{:S(2)}) copy-start(bf16[256,512]{1,0:T(8,128)(2,1)} %param.16) | copy-start | bytes 786436
  7.2 25.1 %copy-start.5 = (bf16[256,512]{1,0:T(8,128)(2,1)S(1)}, bf16[256,512]{1,0:T(8,128)(2,1)}, u32[]{:S(2)}) copy-start(bf16[256,512]{1,0:T(8,128)(2,1)} %param.17) | copy-start | bytes 786436
  7.2 73.4 %all-gather.8.cloned.1.call-start = ((), (), s32[]{:S(2)}) async-start(), calls=%async_computation.5 | async-start | bytes 5242880 | tf_op jit(solution)/shard_map/all_gather | solution.py:18
  9.8 22.6 %copy-start.6 = (bf16[256,512]{1,0:T(8,128)(2,1)S(1)}, bf16[256,512]{1,0:T(8,128)(2,1)}, u32[]{:S(2)}) copy-start(bf16[256,512]{1,0:T(8,128)(2,1)} %param.18) | copy-start | bytes 786436
  9.8 22.7 %copy-start.7 = (bf16[256,512]{1,0:T(8,128)(2,1)S(1)}, bf16[256,512]{1,0:T(8,128)(2,1)}, u32[]{:S(2)}) copy-start(bf16[256,512]{1,0:T(8,128)(2,1)} %param.19) | copy-start | bytes 786436
  9.9 136.0 %all-gather.14.cloned.1.call-start = ((), (), s32[]{:S(2)}) async-start(), calls=%async_computation.8 | async-start | bytes 3932160 | tf_op jit(solution)/shard_map/all_gather | solution.py:18
  31.7 246.9 %all-gather.12.cloned.1.call-start = ((), (), s32[]{:S(2)}) async-start(), calls=%async_computation.7 | async-start | bytes 9175040 | tf_op jit(solution)/shard_map/all_gather | solution.py:18
  66.8 13.8 %copy-start.9 = (f32[4,256]{1,0:T(4,128)S(1)}, f32[4,256]{1,0:T(4,128)}, u32[]{:S(2)}) copy-start(f32[4,256]{1,0:T(4,128)} %param.23) | copy-start | bytes 12292
  69.2 26.9 %copy-start.10 = (f32[8]{0:T(128)S(1)}, f32[8]{0:T(128)}, u32[]{:S(2)}) copy-start(f32[8]{0:T(128)} %param.22) | copy-start | bytes 100
  69.2 228.9 %all-gather.10.cloned.1.call-start = ((), (), s32[]{:S(2)}) async-start(), calls=%async_computation.6 | async-start | bytes 12582912 | tf_op jit(solution)/shard_map/all_gather | solution.py:18
  81.2 14.9 %all-to-all-start.1 = ((f32[4,1,256]{2,1,0:T(1,128)}), f32[4,1,256]{2,1,0:T(1,128)S(1)}, u32[]{:S(2)}, u32[]{:S(2)}) async-start(f32[4,1,256]{2,1,0:T(1,128)} %all_to_all.35), calls=%async_computation.1 | async-start | bytes 8192 | tf_op jit(solution)/shard_map/all_to_all | solution.py:24
  84.5 348.8 %reduce-scatter.2.cloned.1.call-start = ((), (), s32[]{:S(2)}) async-start(), calls=%async_computation.9 | async-start | bytes 9437184 | tf_op jit(solution)/shard_map/reduce_scatter | solution.py:184
  96.0 249.6 %copy-start.1 = (pred[4,256,512]{1,2,0:T(8,128)(4,1)}, pred[4,256,512]{1,2,0:T(8,128)(4,1)S(1)}, u32[]{:S(2)}) copy-start(pred[4,256,512]{1,2,0:T(8,128)(4,1)S(1)} %fusion.14) | copy-start | bytes 1572868
  311.3 31.2 %collective-permute-start = (bf16[2,128,1,128]{1,3,0,2:T(8,128)(2,1)S(1)}, bf16[2,128,1,128]{1,3,0,2:T(8,128)(2,1)}, u32[]{:S(2)}, u32[]{:S(2)}) collective-permute-start(bf16[2,128,1,128]{1,3,0,2:T(8,128)(2,1)S(1)} %slice.102), channel_id=1, source_target_pairs={{0,8},{8,16},{16,24},{1,9},{9,17},{17,25},{2,10},{10,18},{18,26},{... | collective-permute-start | bytes 196616 | tf_op jit(solution)/shard_map/ppermute | solution.py:31
  315.6 27.8 %collective-permute-start.1 = (bf16[2,128,1,128]{1,3,2,0:T(8,128)(2,1)S(1)}, bf16[2,128,1,128]{1,3,2,0:T(8,128)(2,1)}, u32[]{:S(2)}, u32[]{:S(2)}) collective-permute-start(bf16[2,128,1,128]{1,3,2,0:T(8,128)(2,1)S(1)} %slice.105), channel_id=1, source_target_pairs={{8,0},{16,8},{24,16},{9,1},{17,9},{25,17},{10,2},{18,10},{26,18},{... | collective-permute-start | bytes 196616 | tf_op jit(solution)/shard_map/ppermute | solution.py:32
  346.7 6.4 %copy-start = (bf16[16,384,256]{1,2,0:T(8,128)(2,1)S(1)}, bf16[16,384,256]{1,2,0:T(8,128)(2,1)}, u32[]{:S(2)}) copy-start(bf16[16,384,256]{1,2,0:T(8,128)(2,1)} %copy.84) | copy-start | bytes 9437188
  346.7 6.4 %copy-start.8 = (bf16[1024,128]{1,0:T(8,128)(2,1)S(1)}, bf16[1024,128]{1,0:T(8,128)(2,1)}, u32[]{:S(2)}) copy-start(bf16[1024,128]{1,0:T(8,128)(2,1)} %copy.83) | copy-start | bytes 786436
Sparse Core Ops, SparseCore 0:
  10.4 70.1 all-gather.7
  82.2 63.6 all-gather.13
  147.5 131.1 all-gather.11
  280.0 18.0 all-gather.9
  360.0 73.1 reduce-scatter.1

commit v2 on v1

--- a/solution.py
+++ b/solution.py
@@ -1,8 +1,11 @@
+import functools
 import math
 
 import jax
 import jax.numpy as jnp
 from jax import lax
+from jax.experimental import pallas as pl
+from jax.experimental.pallas import tpu as pltpu
 from jax.sharding import Mesh
 from jax.sharding import PartitionSpec as P
 
@@ -10,6 +13,7 @@
 SPAN_RADIUS = 128
 BLOCK = 256
 HIGHEST = lax.Precision.HIGHEST
+MESH = pl.DeviceIdType.MESH
 
 
 def gather(x, axis, dim):
@@ -39,6 +43,273 @@
     return jnp.concatenate(
         [first * cosine - second * sine, second * cosine + first * sine], axis=-1
     ).astype(jnp.bfloat16)
+
+
+def front_kernel(
+    peers, parts, cores,
+    packed, scaled, sums, outp, decay,
+    proj, out_all, sums_all, decay_all,
+    wide, seen,
+    w_recv, up_send, down_send, w_send,
+    x_recv, x_send, swap_send,
+    s_recv, s_send, o_recv, o_send, d_recv, d_send, local,
+):
+    t, h, c = lax.axis_index("t"), lax.axis_index("h"), lax.axis_index("tp")
+    blocks, own, _ = scaled.shape
+
+    def other(d):
+        return lax.rem(h + d, parts)
+
+    def source(d):
+        return lax.rem(h - d + parts, parts)
+
+    barrier = pltpu.get_barrier_semaphore()
+    for d in range(parts):
+        for e in range(cores):
+            if d or e:
+                pl.semaphore_signal(
+                    barrier,
+                    inc=1,
+                    device_id={"h": other(d), "tp": lax.rem(c + e, cores)},
+                    device_id_type=MESH,
+                )
+
+    for d in range(1, peers):
+        pl.semaphore_signal(
+            barrier, inc=1, device_id={"t": lax.rem(t + d, peers)}, device_id_type=MESH
+        )
+    pl.semaphore_wait(barrier, parts * cores + peers - 2)
+
+    def remote(src, dst, send, recv, where):
+        return pltpu.make_async_remote_copy(
+            src_ref=src, dst_ref=dst, send_sem=send, recv_sem=recv,
+            device_id=where, device_id_type=MESH,
+        )
+
+    def upward(b, p, src=None):
+        return remote(
+            wide.at[b, p] if src is None else src,
+            wide.at[b, p], up_send.at[b, p], w_recv.at[b, p], {"t": t + 1},
+        )
+
+    def downward(b, p, src=None):
+        return remote(
+            wide.at[b, p] if src is None else src,
+            wide.at[b, p], down_send.at[b, p], w_recv.at[b, p], {"t": t - 1},
+        )
+
+    def weight_to(d):
+        return remote(
+            packed.at[other(d)], wide.at[t, h], w_send.at[d], w_recv.at[t, h], {"h": other(d)}
+        )
+
+    def place(p, e):
+        return seen.at[pl.ds(e * blocks, blocks), pl.ds(p * own, own)]
+
+    def token_to(d):
+        return remote(scaled, place(h, c), x_send.at[d], x_recv.at[h, c], {"h": other(d)})
+
+    def swap(p, src):
+        return remote(
+            src, place(p, c), swap_send.at[p], x_recv.at[p, c], {"tp": lax.rem(c + 1, cores)}
+        )
+
+    def sum_to(d, e):
+        return remote(
+            sums, sums_all.at[h, c], s_send.at[d, e], s_recv.at[h, c],
+            {"h": other(d), "tp": lax.rem(c + e, cores)},
+        )
+
+    def out_to(d):
+        return remote(
+            outp.at[other(d)], out_all.at[h], o_send.at[d], o_recv.at[h], {"h": other(d)}
+        )
+
+    def decay_to(d):
+        return remote(
+            decay.at[other(d)], decay_all.at[h], d_send.at[d], d_recv.at[h], {"h": other(d)}
+        )
+
+    for d in range(1, parts):
+        weight_to(d).start()
+
+    @pl.when(t < peers - 1)
+    def _():
+        upward(t, h, packed.at[h]).start()
+
+    @pl.when(t > 0)
+    def _():
+        downward(t, h, packed.at[h]).start()
+
+    for d in range(1, parts):
+        token_to(d).start()
+    swap(h, scaled).start()
+    for d in range(1, parts):
+        decay_to(d).start()
+        out_to(d).start()
+    for d in range(parts):
+        for e in range(cores):
+            if d or e:
+                sum_to(d, e).start()
+    mine = (
+        pltpu.make_async_copy(packed.at[h], wide.at[t, h], local.at[0]),
+        pltpu.make_async_copy(scaled, place(h, c), local.at[1]),
+        pltpu.make_async_copy(sums, sums_all.at[h, c], local.at[2]),
+        pltpu.make_async_copy(outp.at[h], out_all.at[h], local.at[3]),
+        pltpu.make_async_copy(decay.at[h], decay_all.at[h], local.at[4]),
+    )
+    for copy in mine:
+        copy.start()
+    proj[...] = jnp.zeros_like(proj)
+
+    @pl.loop(1, parts)
+    def _(d):
+        p = source(d)
+        upward(t, p).wait_recv()
+
+        @pl.when(t < peers - 1)
+        def _():
+            upward(t, p).start()
+
+        @pl.when(t > 0)
+        def _():
+            downward(t, p).start()
+
+    def relay(s, d):
+        p = source(d)
+
+        @pl.when(t - s >= 0)
+        def _():
+            upward(t - s, p).wait_recv()
+
+            @pl.when(t < peers - 1)
+            def _():
+                upward(t - s, p).start()
+
+        @pl.when(t + s < peers)
+        def _():
+            downward(t + s, p).wait_recv()
+
+            @pl.when(t > 0)
+            def _():
+                downward(t + s, p).start()
+
+    @pl.loop(0, parts)
+    def _(d):
+        relay(1, d)
+
+        @pl.when(d < parts - 1)
+        def _():
+            p = source(d + 1)
+            swap(p, place(p, c)).wait_recv()
+            swap(p, place(p, c)).start()
+
+    for copy in mine:
+        copy.wait()
+
+    @pl.loop(0, parts)
+    def _(p):
+        e = lax.rem(c + 1, cores)
+        pltpu.make_async_remote_copy(
+            src_ref=place(p, e), dst_ref=place(p, e),
+            send_sem=swap_send.at[p], recv_sem=x_recv.at[p, e],
+            device_id={"tp": e}, device_id_type=MESH,
+        ).wait_recv()
+
+    def add(b, p):
+        @pl.loop(0, parts)
+        def _(r):
+            at = pl.ds(pl.multiple_of(r * own, own), own)
+            proj[at, :] += jnp.dot(
+                seen[b * parts + p, at, :], wide[b, p], preferred_element_type=jnp.float32
+            )
+
+    @pl.loop(0, peers)
+    def _(s):
+        @pl.loop(0, parts)
+        def _(d):
+            p = source(d)
+
+            @pl.when(s >= 2)
+            def _():
+                relay(s, d)
+
+            @pl.when(t - s >= 0)
+            def _():
+                add(t - s, p)
+
+            @pl.when((s > 0) & (t + s < peers))
+            def _():
+                add(t + s, p)
+
+    @pl.loop(0, peers)
+    def _(b):
+        @pl.loop(0, parts)
+        def _(p):
+            @pl.when((b <= t) & (t < peers - 1))
+            def _():
+                upward(b, p).wait_send()
+
+            @pl.when((b >= t) & (t > 0))
+            def _():
+                downward(b, p).wait_send()
+
+    for p in range(parts):
+        swap(p, place(p, c)).wait_send()
+    for d in range(parts):
+        if d:
+            p = source(d)
+            weight_to(d).wait_send()
+            token_to(d).wait_send()
+            out_to(d).wait_send()
+            decay_to(d).wait_send()
+            remote(
+                outp.at[h], out_all.at[p], o_send.at[d], o_recv.at[p], {"h": p}
+            ).wait_recv()
+            remote(
+                decay.at[h], decay_all.at[p], d_send.at[d], d_recv.at[p], {"h": p}
+            ).wait_recv()
+        for e in range(cores):
+            if d or e:
+                p, q = source(d), lax.rem(c + e, cores)
+                sum_to(d, e).wait_send()
+                remote(
+                    sums, sums_all.at[p, q], s_send.at[d, e], s_recv.at[p, q],
+                    {"h": p, "tp": q},
+                ).wait_recv()
+
+
+def front(packed, scaled, sums, outp, decay):
+    peers, parts, cores = (lax.axis_size(a) for a in ("t", "h", "tp"))
+    own, columns = packed.shape[1:]
+    dma = pltpu.SemaphoreType.DMA
+    vmem = pl.BlockSpec(memory_space=pltpu.VMEM)
+    rows = parts * own
+    return pl.pallas_call(
+        functools.partial(front_kernel, peers, parts, cores),
+        out_shape=(
+            jax.ShapeDtypeStruct((rows, columns), jnp.float32),
+            jax.ShapeDtypeStruct(outp.shape, outp.dtype),
+            jax.ShapeDtypeStruct((parts, cores) + sums.shape, sums.dtype),
+            jax.ShapeDtypeStruct(decay.shape, decay.dtype),
+        ),
+        in_specs=[vmem] * 5,
+        out_specs=[vmem] * 4,
+        scratch_shapes=[
+            pltpu.VMEM((peers, parts, own, columns), jnp.bfloat16),
+            pltpu.VMEM((cores * scaled.shape[0], rows, own), jnp.bfloat16),
+            dma((peers, parts)), dma((peers, parts)), dma((peers, parts)), dma((parts,)),
+            dma((parts, cores)), dma((parts,)), dma((parts,)),
+            dma((parts, cores)), dma((parts, cores)),
+            dma((parts,)), dma((parts,)), dma((parts,)), dma((parts,)), dma((5,)),
+        ],
+        compiler_params=pltpu.CompilerParams(
+            collective_id=0, has_side_effects=True, vmem_limit_bytes=56 * 2**20
+        ),
+        cost_estimate=pl.CostEstimate(
+            flops=10**11, bytes_accessed=2 * 10**7, transcendentals=0
+        ),
+    )(packed, scaled, sums, outp, decay)
 
 
 def attend(query, key, value, sink, offset, total_rows):
@@ -138,16 +409,30 @@
         ],
         axis=2,
     )
-    packed = jnp.moveaxis(packed, 1, 0).reshape(parts * packed.shape[0], packed.shape[2])
-    weight = gather(exchange(packed, "h", 0, 0), "t", 0)
-
+    packed = jnp.moveaxis(packed, 1, 0)
+    out_pack = jnp.concatenate(
+        [w.reshape(parts, w.shape[0] // parts, w.shape[1]) for w in (out_att, out_ret)], axis=1
+    )
     widened = tokens.astype(jnp.float32)
-    sums = lax.all_gather(jnp.sum(widened * widened, axis=1), ("h", "tp"))
-    squares = jnp.sum(sums.reshape(parts, lax.axis_size("tp"), own), axis=1).reshape(rows)
+    sums = jnp.sum(widened * widened, axis=1)
+    scaled = (widened * gain).astype(jnp.bfloat16)
+    cores = lax.axis_size("tp")
+    if parts > 1 and cores == 2 and own % 128 == 0 and packed.shape[1] == own:
+        tiles = jnp.moveaxis(scaled.reshape(own, -1, own), 1, 0)
+        proj, out_own, sums, decay = front(
+            packed, tiles, sums.reshape(-1, 128), out_pack, decay_log.reshape(parts, ret, own)
+        )
+        decay = jnp.moveaxis(decay, 0, 1).reshape(ret, rows)
+    else:
+        flat = packed.reshape(parts * packed.shape[1], packed.shape[2])
+        weight = gather(exchange(flat, "h", 0, 0), "t", 0)
+        whole = gather(gather(scaled, "h", 0), "tp", 1)
+        proj = jnp.dot(whole, weight, preferred_element_type=jnp.float32)
+        out_own = exchange(out_pack, "h", 0, 0)
+        sums = lax.all_gather(sums, ("h", "tp"))
+        decay = exchange(decay_log, "h", 0, 1)
+    squares = jnp.sum(sums.reshape(parts, cores, own), axis=1).reshape(rows)
     inverse = lax.rsqrt(squares / width + 1e-06)[:, None]
-    scaled = (widened * gain).astype(jnp.bfloat16)
-    whole = gather(gather(scaled, "h", 0), "tp", 1)
-    proj = jnp.dot(whole, weight, preferred_element_type=jnp.float32)
 
     edges = [att, kv, kv, ret, ret, ret]
     starts = [sum(edges[:i]) * HEAD_DIM for i in range(6)]
@@ -170,12 +455,9 @@
     att_out, logs = attend(
         att_query.reshape(rows, kv, group, HEAD_DIM), att_key, att_value, logits, offset, total_rows
     )
-    ret_out = retain(ret_query, ret_key, ret_value, exchange(decay_log, "h", 0, 1))
-
-    out_pack = jnp.concatenate(
-        [w.reshape(parts, w.shape[0] // parts, w.shape[1]) for w in (out_att, out_ret)], axis=1
-    )
-    out_wide = gather(exchange(out_pack, "h", 0, 0), "t", 0)
+    ret_out = retain(ret_query, ret_key, ret_value, decay)
+
+    out_wide = gather(out_own, "t", 0)
     depth = out_wide.shape[1]
     out_wide = jnp.moveaxis(out_wide, 0, 1).reshape(depth, -1)
     mixed = jnp.dot(

time: 440 us -> 324 us (0.74)
  waiting for transfers between devices: 270 us -> 76.9 us
  Pallas kernels: 0 us -> 135 us
  blocking collectives: 89 us -> 33.5 us
  matrix products: 28.2 us -> 16.4 us
  local copies, waits for them, and re-layouts: 16.1 us -> 26.8 us
  starting transfers between devices: 9.02 us -> 3.27 us
    all_gather x4 -> x1, waiting for transfers between devices: 205 us -> 14.8 us  [gather(): return lax.all_gather(x, axis, axis=dim, tiled=True)]
    pallas_call x0 -> x1, Pallas kernels: none -> 135 us  [front(): pl.pallas_call(functools.partial(front_kernel, peers, parts, cores), out_...]
    all_to_all x3 -> x1, blocking collectives: 62.6 us -> 7.53 us  [exchange(): return lax.all_to_all(x, axis, split, concat, tiled=True)]
    dot_general x1 -> x0, matrix products: 11.4 us -> none  [shards(): proj = jnp.dot(whole, weight, preferred_element_type=jnp.float32)]
    all_gather x1 -> x0, blocking collectives: 9.34 us -> none  [shards(): sums = lax.all_gather(jnp.sum(widened * widened, axis=1), ('h', 'tp'))]
    all_gather x1, blocking collectives: 17.1 us -> 26 us  [retain(): seen = lax.all_gather(sent, 't', axis=0)]
    reshape x1 -> x9, local copies, waits for them, and re-layouts: 0.01 us -> 6.59 us  [the longest x6 2.38 us: shards(): w.reshape(w.shape[0], parts, w.shape[1] // parts)]
    unnamed x35 -> x33, local copies, waits for them, and re-layouts: 2.15 us -> 8.61 us
  transfers between devices with their start and end apart: 8 -> 4, of which waited for: 5 -> 2; matrix products, arithmetic and copies ran while one was open for 5% -> 9% of each run, Pallas kernels for 0% -> 0%
where the time goes in v2:
time: 324 us; the launch traced here: 323 us
  Pallas kernels  135 us (42%)
  waiting for transfers between devices  76.9 us (24%)
  blocking collectives  33.5 us (10%)
  local copies, waits for them, and re-layouts  26.8 us (8%)
  matrix products  16.4 us (5%)
  between operations  15.9 us (5%)
  other arithmetic  14.6 us (5%)
  starting transfers between devices  3.27 us (1%)
    pallas_call x1, Pallas kernels, front(): pl.pallas_call(functools.partial(front_kernel, peers, parts, cores), out_...  135 us
    reduce_scatter x1, waiting for transfers between devices, shards(): lax.psum_scatter(mixed, ('h', 'tp'), scatter_dimension=0, tiled=True)  62.1 us
    all_gather x1, blocking collectives, retain(): seen = lax.all_gather(sent, 't', axis=0)  26 us
    all_gather x1, waiting for transfers between devices, gather(): return lax.all_gather(x, axis, axis=dim, tiled=True)  14.8 us
    unnamed x33, local copies, waits for them, and re-layouts  8.61 us
    dot_general x1, matrix products, shards(): jnp.dot(jnp.concatenate([att_out, ret_out], axis=1), out_wide, preferred_...  7.78 us
    all_to_all x1, blocking collectives, exchange(): return lax.all_to_all(x, axis, split, concat, tiled=True)  7.53 us
  transfers between devices with their start and end apart: 4, of which 2 were waited for; matrix products, arithmetic and copies ran while one was open for 9% of the time, Pallas kernels for 0%

profile of v2, /device:TPU:0, one launch (start us, length us, event | category | flops | bytes accessed | tf_op | source)
XLA Modules:
  0.0 322.8 jit_solution(4144203219415570787)
XLA Ops:
  7.2 1.3 reshape.725.decay
  8.6 1.1 copy.74
  9.7 0.2 copy.80
  9.8 1.1 copy.75
  10.9 0.2 copy.81
  11.1 1.1 copy.76
  12.2 0.2 copy.82
  12.4 1.1 copy.77
  13.5 0.8 copy.83
  14.3 0.1 copy.78
  14.5 0.8 copy.84
  15.3 0.2 copy.73
  15.5 0.2 copy.79
  15.7 1.5 copy.85
  17.2 0.9 fusion.9
  18.2 1.3 copy.86
  19.5 2.1 pad_maximum_fusion.1.outp
  22.0 1.2 copy-done.6
  23.3 135.4 %shard_map.131 = (f32[1024,896]{1,0:T(8,128)}, bf16[4,384,256]{2,1,0:T(8,128)(2,1)}, f32[4,2,2,128]{3,2,1,0:T(2,128)}, f32[4,1,256]{2,1,0:T(1,128)}) custom-call(bf16[4,256,896]{2,1,0:T(8,128)(2,1)} %bitcast.171, bf16[8,256,256]{2,1,0:T(8,128)(2,1)} %bitcast.162, f32[2,128]{1,0:T(2,128)} %bitcast.179, bf16[4,384,256]{2,1,0:T(8,128)(2,1)} %pad_maximum_fusion.1.outp, ...), custom_call_target="tpu_custom_call" | custom-call | flops 99999997952 | bytes 20000000 | tf_op jit(solution)/shard_map/pallas_call | solution.py:288
  158.7 0.7 reduce_sum.75
  159.5 2.0 multiply_bitcast_fusion
  161.5 2.4 fusion.53
  164.0 0.2 fusion.76
  164.1 1.9 collective-permute-start
  166.0 0.2 pad_maximum_fusion.2
  166.2 0.6 slice.103
  166.8 1.3 collective-permute-start.1
  168.1 0.3 reduce-window.6
  168.4 0.2 slice_reduce_fusion
  168.6 0.6 slice.108
  169.2 0.2 reduce-window.9
  169.4 0.6 slice.109
  171.4 0.8 convolution_bitcast_fusion.2
  172.2 0.7 convolution_bitcast_fusion.3
  173.0 26.0 %all-gather = f32[4,264,128]{2,1,0:T(8,128)S(1)} all-gather(f32[1,264,128]{2,1,0:T(8,128)S(1)} %maximum_maximum_fusion), channel_id=2, replica_groups=mesh['t'=4,'h'=4,'tp'=2] {'t'}, dimensions={0}, use_global_device_ids=true | all-gather | bytes 675840 | tf_op jit(solution)/shard_map/all_gather | solution.py:358
  199.2 0.2 select_reduce_fusion
  199.3 0.7 fusion.65
  200.2 0.4 fusion.28
  200.6 3.3 %fusion.19 = f32[1,128,1024]{2,1,0:T(8,128)S(1)} fusion(bf16[1024,128]{1,0:T(8,128)(2,1)S(1)} %get-tuple-element.16, f32[1024,1024]{1,0:T(8,128)S(1)} %fusion.65, f32[1024]{0:T(1024)S(1)} %get-tuple-element.13), kind=kOutput, calls=%fused_computation.24 | convolution fusion | flops 1614807040 | bytes 4984832 | tf_op jit(solution)/shard_map/hqk,khd->qhd/dot_general | solution.py:379
  203.9 0.5 fusion.64
  204.5 2.3 slice.86
  206.7 1.6 copy.104
  208.5 1.0 multiply_cosine_fusion.1
  209.6 0.1 broadcast_multiply_fusion
  209.8 0.2 subtract_convert_fusion
  209.9 1.0 fusion.14
  211.0 0.2 concatenate.53
  211.2 0.3 copy.92
  211.5 0.2 concatenate.54
  211.7 1.1 copy.93
  212.7 0.8 copy.97
  213.8 0.9 fusion.49
  214.7 0.1 pad_maximum_fusion
  214.9 1.0 fusion.7
  215.9 1.0 fusion.6
  217.0 1.3 fusion.22
  218.3 0.4 copy.96
  218.7 0.9 copy.107
  219.6 14.8 %all-gather.3.cloned.1.call-done = bf16[16,384,256]{2,1,0:T(8,128)(2,1)} async-done(((bf16[4,384,256]{2,1,0:T(8,128)(2,1)}), bf16[16,384,256]{2,1,0:T(8,128)(2,1)}) %all-gather.3.cloned.1.call-update) | async-done | bytes 3145744 | tf_op jit(solution)/shard_map/all_gather | solution.py:22
  234.4 3.4 %copy.98 = bf16[16,384,256]{1,2,0:T(8,128)(2,1)S(1)} copy(bf16[16,384,256]{2,1,0:T(8,128)(2,1)} %all-gather.3.cloned.1.call-done) | data formatting | bytes 6291456 | tf_op jit(solution)/shard_map/all_gather | solution.py:22
  237.8 7.8 %convolution_convert_fusion = bf16[1024,4096]{1,0:T(8,128)(2,1)} fusion(bf16[384,4096]{0,1:T(8,128)(2,1)S(1)} %bitcast.157, bf16[1024,128]{1,0:T(8,128)(2,1)S(1)} %copy-done.5, bf16[1024,256]{1,0:T(8,128)(2,1)} %bitcast.169), kind=kOutput, calls=%fused_computation | convolution fusion | flops 3226992640 | bytes 12320768 | tf_op jit(solution)/shard_map/dot_general | solution.py:463
  245.7 7.5 %all_to_all.19 = f32[2,4,256]{2,0,1:T(2,128)S(1)} all-to-all(f32[2,4,256]{2,0,1:T(2,128)S(1)} %fusion.56), channel_id=1, replica_groups=mesh['t'=4,'h'=4,'tp'=2] {'h'}, dimensions={1} | all-to-all | bytes 16384 | tf_op jit(solution)/shard_map/all_to_all | solution.py:28
  253.2 0.6 all_to_all.17
  253.8 62.1 %reduce-scatter.2.cloned.1.call-done = bf16[128,4096]{1,0:T(8,128)(2,1)} async-done(((bf16[1024,4096]{1,0:T(8,128)(2,1)}), bf16[128,4096]{1,0:T(8,128)(2,1)}) %reduce-scatter.2.cloned.1.call-update) | async-done | bytes 1048592 | tf_op jit(solution)/shard_map/reduce_scatter | solution.py:466
  (60 shorter events, 1.8 us)
Async XLA Ops:
  7.2 7.2 %copy-start.4 = (bf16[256,512]{1,0:T(8,128)(2,1)S(1)}, bf16[256,512]{1,0:T(8,128)(2,1)}, u32[]{:S(2)}) copy-start(bf16[256,512]{1,0:T(8,128)(2,1)} %param.19) | copy-start | bytes 786436
  7.2 8.1 %copy-start.3 = (bf16[256,1024]{1,0:T(8,128)(2,1)S(1)}, bf16[256,1024]{1,0:T(8,128)(2,1)}, u32[]{:S(2)}) copy-start(bf16[256,1024]{1,0:T(8,128)(2,1)} %param.14) | copy-start | bytes 1572868
  7.2 227.2 %all-gather.3.cloned.1.call-start = ((), (), s32[]{:S(2)}) async-start(), calls=%async_computation.2 | async-start | bytes 3932160 | tf_op jit(solution)/shard_map/all_gather | solution.py:22
  11.1 6.1 %copy-start.7 = (f32[2048]{0:T(1024)S(1)}, f32[2048]{0:T(1024)}, u32[]{:S(2)}) copy-start(f32[2048]{0:T(1024)} %param.13) | copy-start | bytes 24580
  18.2 3.7 %copy-start = (bf16[256,4,128]{2,0,1:T(8,128)(2,1)S(1)}, bf16[256,4,128]{2,0,1:T(8,128)(2,1)}, u32[]{:S(2)}) copy-start(bf16[256,4,128]{2,0,1:T(8,128)(2,1)} %copy.83) | copy-start | bytes 786436
  18.2 3.8 %copy-start.1 = (bf16[256,4,128]{2,0,1:T(8,128)(2,1)S(1)}, bf16[256,4,128]{2,0,1:T(8,128)(2,1)}, u32[]{:S(2)}) copy-start(bf16[256,4,128]{2,0,1:T(8,128)(2,1)} %copy.84) | copy-start | bytes 786436
  22.0 1.3 copy-start.6
  158.6 157.3 %reduce-scatter.2.cloned.1.call-start = ((), (), s32[]{:S(2)}) async-start(), calls=%async_computation.3 | async-start | bytes 9437184 | tf_op jit(solution)/shard_map/reduce_scatter | solution.py:466
  159.5 8.7 %copy-start.8 = (f32[4,1,256]{2,1,0:T(1,128)S(1)}, f32[4,1,256]{2,1,0:T(1,128)}, u32[]{:S(2)}) copy-start(f32[4,1,256]{2,1,0:T(1,128)} %get-tuple-element.8) | copy-start | bytes 12292
  164.1 49.6 %collective-permute-start = (bf16[2,128,1,128]{3,1,0,2:T(8,128)(2,1)S(1)}, bf16[2,128,1,128]{3,1,0,2:T(8,128)(2,1)}, u32[]{:S(2)}, u32[]{:S(2)}) collective-permute-start(bf16[2,128,1,128]{3,1,0,2:T(8,128)(2,1)S(1)} %slice.100), channel_id=1, source_target_pairs={{0,8},{8,16},{16,24},{1,9},{9,17},{17,25},{2,10},{10,18},{18,26},{... | collective-permute-start | bytes 196616 | tf_op jit(solution)/shard_map/ppermute | solution.py:35
  166.8 46.8 %collective-permute-start.1 = (bf16[2,128,1,128]{3,1,2,0:T(8,128)(2,1)}, bf16[2,128,1,128]{3,1,2,0:T(8,128)(2,1)S(1)}, u32[]{:S(2)}, u32[]{:S(2)}) collective-permute-start(bf16[2,128,1,128]{3,1,2,0:T(8,128)(2,1)} %slice.103), channel_id=1, source_target_pairs={{8,0},{16,8},{24,16},{9,1},{17,9},{25,17},{10,2},{18,10},{26,18},{... | collective-permute-start | bytes 196616 | tf_op jit(solution)/shard_map/ppermute | solution.py:36
  209.6 4.0 %copy-start.9 = (f32[8]{0:T(128)S(1)}, f32[8]{0:T(128)}, u32[]{:S(2)}) copy-start(f32[8]{0:T(128)} %param.22) | copy-start | bytes 100
  212.7 2.1 copy-start.2
  218.7 19.1 %copy-start.5 = (bf16[1024,128]{1,0:T(8,128)(2,1)S(1)}, bf16[1024,128]{1,0:T(8,128)(2,1)}, u32[]{:S(2)}) copy-start(bf16[1024,128]{1,0:T(8,128)(2,1)} %copy.97) | copy-start | bytes 786436
Sparse Core Ops, SparseCore 0:
  158.8 75.5 all-gather.2
  245.7 70.1 reduce-scatter.1

commit v3 on v2

--- a/solution.py
+++ b/solution.py
@@ -312,6 +312,128 @@
     )(packed, scaled, sums, outp, decay)
 
 
+def back_kernel(
+    parts, cores, mixers, wide, logs, mixed, logs_all,
+    give, take, mine, total, seen,
+    give_send, take_recv, total_send, seen_recv, l_send, l_recv, local,
+):
+    h, c = lax.axis_index("h"), lax.axis_index("tp")
+    partner = lax.rem(c + 1, cores)
+    half = mixed.shape[0]
+    count, _, tile = wide.shape
+
+    def other(d):
+        return lax.rem(h + d, parts)
+
+    barrier = pltpu.get_barrier_semaphore()
+    for d in range(1, parts):
+        pl.semaphore_signal(barrier, inc=1, device_id={"h": other(d)}, device_id_type=MESH)
+    pl.semaphore_signal(barrier, inc=1, device_id={"tp": partner}, device_id_type=MESH)
+    pl.semaphore_wait(barrier, parts)
+
+    def remote(src, dst, send, recv, where):
+        return pltpu.make_async_remote_copy(
+            src_ref=src, dst_ref=dst, send_sem=send, recv_sem=recv,
+            device_id=where, device_id_type=MESH,
+        )
+
+    def swap(d):
+        return remote(give.at[d], take.at[d], give_send.at[d], take_recv.at[d], {"tp": partner})
+
+    def scatter(d):
+        return remote(
+            total.at[d], seen.at[d], total_send.at[d], seen_recv.at[d], {"h": other(d)}
+        )
+
+    def log_to(d):
+        return remote(
+            logs.at[other(d)], logs_all.at[h], l_send.at[d], l_recv.at[h], {"h": other(d)}
+        )
+
+    for d in range(1, parts):
+        log_to(d).start()
+    own_logs = pltpu.make_async_copy(logs.at[h], logs_all.at[h], local.at[0])
+    own_logs.start()
+
+    def project(d):
+        at = pl.ds(pl.multiple_of(other(d) * 2 * half, 2 * half), 2 * half)
+
+        @pl.loop(0, count)
+        def _(j):
+            columns = pl.ds(pl.multiple_of(j * tile, tile), tile)
+            part = jnp.dot(mixers[at, :], wide[j], preferred_element_type=jnp.float32)
+            low, high = part[:half], part[half:]
+            give[d, :, columns] = jnp.where(c == 0, high, low).astype(give.dtype)
+            mine[d, :, columns] = jnp.where(c == 0, low, high)
+
+    def settle(d):
+        swap(d).wait_recv()
+        total[d] = (mine[d] + take[d].astype(jnp.float32)).astype(total.dtype)
+        scatter(d).start()
+
+    @pl.loop(1, parts + 1)
+    def _(i):
+        d = lax.rem(i, parts)
+        project(d)
+        swap(d).start()
+
+        @pl.when(i > 1)
+        def _():
+            settle(i - 1)
+
+    swap(0).wait_recv()
+    mine[0] = mine[0] + take[0].astype(jnp.float32)
+
+    @pl.loop(1, parts)
+    def _(d):
+        scatter(d).wait_recv()
+        mine[0] += seen[d].astype(jnp.float32)
+
+    mixed[...] = mine[0].astype(mixed.dtype)
+
+    own_logs.wait()
+    for d in range(parts):
+        swap(d).wait_send()
+        if d:
+            scatter(d).wait_send()
+            log_to(d).wait_send()
+            p = lax.rem(h - d + parts, parts)
+            remote(
+                logs.at[h], logs_all.at[p], l_send.at[d], l_recv.at[p], {"h": p}
+            ).wait_recv()
+
+
+def back(mixers, wide, logs):
+    parts, cores = lax.axis_size("h"), lax.axis_size("tp")
+    half = mixers.shape[0] // parts // cores
+    columns = wide.shape[0] * wide.shape[2]
+    dma = pltpu.SemaphoreType.DMA
+    vmem = pl.BlockSpec(memory_space=pltpu.VMEM)
+    block = (parts, half, columns)
+    return pl.pallas_call(
+        functools.partial(back_kernel, parts, cores),
+        out_shape=(
+            jax.ShapeDtypeStruct((half, columns), jnp.bfloat16),
+            jax.ShapeDtypeStruct(logs.shape, logs.dtype),
+        ),
+        in_specs=[vmem] * 3,
+        out_specs=[vmem] * 2,
+        scratch_shapes=[
+            pltpu.VMEM(block, jnp.bfloat16), pltpu.VMEM(block, jnp.bfloat16),
+            pltpu.VMEM(block, jnp.float32),
+            pltpu.VMEM(block, jnp.bfloat16), pltpu.VMEM(block, jnp.bfloat16),
+        ]
+        + [dma((parts,))] * 6
+        + [dma((1,))],
+        compiler_params=pltpu.CompilerParams(
+            collective_id=1, has_side_effects=True, vmem_limit_bytes=56 * 2**20
+        ),
+        cost_estimate=pl.CostEstimate(
+            flops=5 * 10**10, bytes_accessed=2 * 10**7, transcendentals=0
+        ),
+    )(mixers, wide, logs)
+
+
 def attend(query, key, value, sink, offset, total_rows):
     rows, kv, group, _ = query.shape
     ext = halo(jnp.stack([key, value]), "t", SPAN_RADIUS)
@@ -417,7 +539,8 @@
     sums = jnp.sum(widened * widened, axis=1)
     scaled = (widened * gain).astype(jnp.bfloat16)
     cores = lax.axis_size("tp")
-    if parts > 1 and cores == 2 and own % 128 == 0 and packed.shape[1] == own:
+    fused = parts > 1 and cores == 2 and own % 128 == 0 and packed.shape[1] == own
+    if fused:
         tiles = jnp.moveaxis(scaled.reshape(own, -1, own), 1, 0)
         proj, out_own, sums, decay = front(
             packed, tiles, sums.reshape(-1, 128), out_pack, decay_log.reshape(parts, ret, own)
@@ -458,11 +581,14 @@
     ret_out = retain(ret_query, ret_key, ret_value, decay)
 
     out_wide = gather(out_own, "t", 0)
+    mixers = jnp.concatenate([att_out, ret_out], axis=1)
+    if fused:
+        sent = jnp.moveaxis(logs.reshape(att, parts, own), 1, 0)
+        mixed, seen = back(mixers, out_wide, sent)
+        return mixed, seen.reshape(parts * att, own)
     depth = out_wide.shape[1]
     out_wide = jnp.moveaxis(out_wide, 0, 1).reshape(depth, -1)
-    mixed = jnp.dot(
-        jnp.concatenate([att_out, ret_out], axis=1), out_wide, preferred_element_type=jnp.float32
-    ).astype(jnp.bfloat16)
+    mixed = jnp.dot(mixers, out_wide, preferred_element_type=jnp.float32).astype(jnp.bfloat16)
     mixed = lax.psum_scatter(mixed, ("h", "tp"), scatter_dimension=0, tiled=True)
     return mixed, exchange(logs, "h", 1, 0)
 

time: 324 us -> 310 us (0.957)
  Pallas kernels: 135 us -> 196 us
  waiting for transfers between devices: 76.9 us -> 22.8 us
  matrix products: 16.4 us -> 8.1 us
  blocking collectives: 33.5 us -> 26 us
  local copies, waits for them, and re-layouts: 26.8 us -> 22 us
    reduce_scatter x1 -> x0, waiting for transfers between devices: 62.1 us -> none  [shards(): lax.psum_scatter(mixed, ('h', 'tp'), scatter_dimension=0, tiled=True)]
    pallas_call x0 -> x1, Pallas kernels: none -> 60.2 us  [back(): pl.pallas_call(functools.partial(back_kernel, parts, cores), out_shape=(j...]
    all_gather x1, waiting for transfers between devices: 14.8 us -> 22.8 us  [gather(): return lax.all_gather(x, axis, axis=dim, tiled=True)]
    dot_general x1 -> x0, matrix products: 7.78 us -> none  [shards(): jnp.dot(jnp.concatenate([att_out, ret_out], axis=1), out_wide, preferred_...]
    all_to_all x1 -> x0, blocking collectives: 7.53 us -> none  [exchange(): return lax.all_to_all(x, axis, split, concat, tiled=True)]
    all_gather x1 -> x0, local copies, waits for them, and re-layouts: 3.42 us -> none  [gather(): return lax.all_gather(x, axis, axis=dim, tiled=True)]
    unnamed x33 -> x38, local copies, waits for them, and re-layouts: 8.61 us -> 9.29 us
  transfers between devices with their start and end apart: 4 -> 3, of which waited for: 2 -> 1; matrix products, arithmetic and copies ran while one was open for 9% -> 8% of each run, Pallas kernels for 0% -> 0%
where the time goes in v3:
time: 310 us; the launch traced here: 308 us
  Pallas kernels  196 us (63%)
  blocking collectives  26 us (8%)
  waiting for transfers between devices  22.8 us (7%)
  local copies, waits for them, and re-layouts  22 us (7%)
  between operations  15.8 us (5%)
  other arithmetic  15.5 us (5%)
  matrix products  8.1 us (3%)
    pallas_call x1, Pallas kernels, front(): pl.pallas_call(functools.partial(front_kernel, peers, parts, cores), out_...  135 us
    pallas_call x1, Pallas kernels, back(): pl.pallas_call(functools.partial(back_kernel, parts, cores), out_shape=(j...  60.2 us
    all_gather x1, blocking collectives, retain(): seen = lax.all_gather(sent, 't', axis=0)  26 us
    all_gather x1, waiting for transfers between devices, gather(): return lax.all_gather(x, axis, axis=dim, tiled=True)  22.8 us
    unnamed x38, local copies, waits for them, and re-layouts  9.29 us
  transfers between devices with their start and end apart: 3, of which 1 were waited for; matrix products, arithmetic and copies ran while one was open for 8% of the time, Pallas kernels for 0%

profile of v3, /device:TPU:0, one launch (start us, length us, event | category | flops | bytes accessed | tf_op | source)
XLA Modules:
  0.0 308.4 jit_solution(16821674189623965535)
XLA Ops:
  7.2 1.5 copy.90
  8.8 1.7 fusion.9
  10.5 1.3 copy.91
  11.8 0.2 copy.78
  12.0 0.2 copy.84
  12.2 0.9 constant_dynamic-update-slice_fusion.5
  13.2 0.2 copy.85
  13.6 0.2 copy.86
  13.8 0.1 copy.81
  13.9 0.2 copy.87
  14.2 0.2 copy.88
  14.5 0.2 copy.89
  14.7 0.6 reshape.720.decay
  15.3 0.8 constant_dynamic-update-slice_fusion.4
  16.1 0.8 constant_dynamic-update-slice_fusion.3
  16.8 0.7 constant_dynamic-update-slice_fusion.2
  17.6 0.8 constant_dynamic-update-slice_fusion.1
  18.3 0.8 constant_dynamic-update-slice_fusion
  19.1 1.0 pad_maximum_fusion.1.outp
  20.1 135.4 %shard_map.131 = (f32[1024,896]{1,0:T(8,128)}, bf16[4,384,256]{2,1,0:T(8,128)(2,1)}, f32[4,2,2,128]{3,2,1,0:T(2,128)}, f32[4,1,256]{2,1,0:T(1,128)}) custom-call(bf16[4,256,896]{2,1,0:T(8,128)(2,1)} %bitcast.167, bf16[8,256,256]{2,1,0:T(8,128)(2,1)} %bitcast.159, f32[2,128]{1,0:T(2,128)} %bitcast.174, bf16[4,384,256]{2,1,0:T(8,128)(2,1)} %pad_maximum_fusion.1.outp, ...), custom_call_target="tpu_custom_call" | custom-call | flops 99999997952 | bytes 20000000 | tf_op jit(solution)/shard_map/pallas_call | solution.py:288
  155.5 0.7 reduce_sum.75
  156.3 2.0 multiply_bitcast_fusion
  158.3 2.4 fusion.50
  160.8 0.2 fusion.71
  160.9 1.3 collective-permute-start
  162.2 0.2 pad_maximum_fusion.3
  162.4 1.3 collective-permute-start.1
  163.8 0.3 reduce-window.6
  164.1 0.2 slice_reduce_fusion
  164.3 0.2 reduce-window.9
  164.6 0.6 slice.109
  165.2 0.6 slice.108
  167.1 0.8 convolution_bitcast_fusion.2
  167.9 0.7 convolution_bitcast_fusion.3
  168.7 26.0 %all-gather = f32[4,264,128]{2,1,0:T(8,128)S(1)} all-gather(f32[1,264,128]{2,1,0:T(8,128)S(1)} %maximum_maximum_fusion), channel_id=2, replica_groups=mesh['t'=4,'h'=4,'tp'=2] {'t'}, dimensions={0}, use_global_device_ids=true | all-gather | bytes 675840 | tf_op jit(solution)/shard_map/all_gather | solution.py:480
  194.9 0.2 select_reduce_fusion
  195.1 0.7 fusion.61
  195.9 0.4 fusion.28
  196.3 2.8 fusion.19
  199.0 0.5 fusion.60
  199.6 2.3 slice.86
  201.9 1.6 copy.113
  203.4 0.4 multiply_reduce_fusion
  203.9 1.0 multiply_cosine_fusion.1
  204.9 0.3 fusion.42
  205.2 0.1 broadcast_multiply_fusion
  205.4 0.2 subtract_convert_fusion
  205.5 1.0 fusion.14
  206.6 0.2 concatenate.53
  206.8 0.3 copy.97
  207.1 0.2 concatenate.54
  207.3 1.1 copy.98
  208.6 0.1 pad_maximum_fusion
  208.8 0.6 copy-done.1
  209.4 1.0 fusion.7
  210.5 1.0 fusion.6
  211.5 1.3 fusion.22
  212.8 0.4 copy.101
  213.3 1.0 pad_maximum_fusion.2.mixers
  214.3 0.7 fusion.53.logs
  215.0 22.8 %all-gather.3.cloned.1.call-done.wide = bf16[16,384,256]{2,1,0:T(8,128)(2,1)} async-done(((bf16[4,384,256]{2,1,0:T(8,128)(2,1)}), bf16[16,384,256]{2,1,0:T(8,128)(2,1)}) %all-gather.3.cloned.1.call-update) | async-done | bytes 3145744 | tf_op jit(solution)/shard_map/all_gather | solution.py:22
  237.7 60.2 %shard_map.132 = (bf16[128,4096]{1,0:T(8,128)(2,1)}, f32[4,2,256]{2,1,0:T(2,128)}) custom-call(bf16[1024,384]{1,0:T(8,128)(2,1)} %pad_maximum_fusion.2.mixers, bf16[16,384,256]{2,1,0:T(8,128)(2,1)} %all-gather.3.cloned.1.call-done.wide, f32[4,2,256]{2,1,0:T(2,128)} %fusion.53.logs), custom_call_target="tpu_custom_call" | custom-call | flops 49999998976 | bytes 20000000 | tf_op jit(solution)/shard_map/pallas_call | solution.py:413
  297.9 1.3 reshape.734
  299.2 2.3 copy.123
  (60 shorter events, 1.9 us)
Async XLA Ops:
  7.2 4.6 %copy-start.2 = (bf16[256,1024]{1,0:T(8,128)(2,1)S(1)}, bf16[256,1024]{1,0:T(8,128)(2,1)}, u32[]{:S(2)}) copy-start(bf16[256,1024]{1,0:T(8,128)(2,1)} %param.14) | copy-start | bytes 1572868
  7.2 230.6 %all-gather.3.cloned.1.call-start = ((), (), s32[]{:S(2)}) async-start(), calls=%async_computation | async-start | bytes 3932160 | tf_op jit(solution)/shard_map/all_gather | solution.py:22
  8.8 4.3 %copy-start.3 = (bf16[256,512]{1,0:T(8,128)(2,1)S(1)}, bf16[256,512]{1,0:T(8,128)(2,1)}, u32[]{:S(2)}) copy-start(bf16[256,512]{1,0:T(8,128)(2,1)} %param.15) | copy-start | bytes 786436
  10.5 2.9 copy-start.4
  10.5 3.3 %copy-start.5 = (bf16[256,512]{1,0:T(8,128)(2,1)S(1)}, bf16[256,512]{1,0:T(8,128)(2,1)}, u32[]{:S(2)}) copy-start(bf16[256,512]{1,0:T(8,128)(2,1)} %param.17) | copy-start | bytes 786436
  11.8 2.3 copy-start.6
  11.8 2.6 copy-start.7
  12.0 2.7 copy-start.9
  13.2 5.9 %copy-start = (bf16[1024,256]{1,0:T(8,128)(2,1)S(1)}, bf16[1024,256]{1,0:T(8,128)(2,1)}, u32[]{:S(2)}) copy-start(bf16[1024,256]{1,0:T(8,128)(2,1)} %param.20) | copy-start | bytes 1572868
  13.2 5.9 %copy-start.8 = (bf16[512,256]{1,0:T(8,128)(2,1)S(1)}, bf16[512,256]{1,0:T(8,128)(2,1)}, u32[]{:S(2)}) copy-start(bf16[512,256]{1,0:T(8,128)(2,1)} %param.21) | copy-start | bytes 786436
  158.3 5.5 %copy-start.10 = (f32[4,1,256]{2,1,0:T(1,128)S(1)}, f32[4,1,256]{2,1,0:T(1,128)}, u32[]{:S(2)}) copy-start(f32[4,1,256]{2,1,0:T(1,128)} %get-tuple-element.10) | copy-start | bytes 12292
  160.9 47.6 %collective-permute-start = (bf16[2,128,1,128]{3,1,0,2:T(8,128)(2,1)S(1)}, bf16[2,128,1,128]{3,1,0,2:T(8,128)(2,1)S(1)}, u32[]{:S(2)}, u32[]{:S(2)}) collective-permute-start(bf16[2,128,1,128]{3,1,0,2:T(8,128)(2,1)S(1)} %slice.100), channel_id=1, source_target_pairs={{0,8},{8,16},{16,24},{1,9},{9,17},{17,25},{2,10},{10,18},{18,26},{... | collective-permute-start | bytes 196616 | tf_op jit(solution)/shard_map/ppermute | solution.py:35
  162.4 46.0 %collective-permute-start.1 = (bf16[2,128,1,128]{3,1,2,0:T(8,128)(2,1)S(1)}, bf16[2,128,1,128]{3,1,2,0:T(8,128)(2,1)S(1)}, u32[]{:S(2)}, u32[]{:S(2)}) collective-permute-start(bf16[2,128,1,128]{3,1,2,0:T(8,128)(2,1)S(1)} %slice.103), channel_id=1, source_target_pairs={{8,0},{16,8},{24,16},{9,1},{17,9},{25,17},{10,2},{18,10},{26,18},{... | collective-permute-start | bytes 196616 | tf_op jit(solution)/shard_map/ppermute | solution.py:36
  205.2 3.1 %copy-start.11 = (f32[8]{0:T(128)S(1)}, f32[8]{0:T(128)}, u32[]{:S(2)}) copy-start(f32[8]{0:T(128)} %param.22) | copy-start | bytes 100
  208.3 1.0 copy-start.1
Sparse Core Ops, SparseCore 0:
  163.9 73.8 all-gather.2
